TPU v7x, 32 devices: a whole 2x2x4 slice. The times are simulated.
32 devices in a mesh: sp: 16 (over z, y, x), tp: 2 (over core).
Axes of the slice: x: 2, y: 2, z: 4, core: 2. Of those that a mesh axis runs over, the one named last changes fastest.
Arguments:
- hidden: bfloat16 [3072, 2048], P('sp')
- norm_gain: float32 [2048], replicated, may hold values from 0.1 to 1.9
- query_weight: bfloat16 [2048, 1024], P(None, 'tp'), may hold values from -0.125 to 0.125
- key_weight: bfloat16 [2048, 256], replicated, may hold values from -0.125 to 0.125
- value_weight: bfloat16 [2048, 256], replicated, may hold values from -0.125 to 0.125
- head_bias: float32 [16], P('tp'), may hold values from -10 to -3.5
- output_weight: bfloat16 [1024, 2048], P('tp'), may hold values from -0.1875 to 0.1875
Outputs:
- mixed: bfloat16 [3072, 2048], P('sp')
All inputs are finite; a program needn't handle non-finite values.
Results may differ from a plain program's by a relative error of at most 0.014.
Values may be sent and summed in bfloat16 or wider, within the bound.
A program may use at most 64 MiB of HBM per device.

v0:
```python
import math

import jax
import jax.numpy as jnp
from jax import lax
from jax.sharding import PartitionSpec as P

HEADS = 16
KV_HEADS = 4
HEAD_DIM = 64


def local(hidden, norm_gain, query_weight, key_weight, value_weight, head_bias, output_weight):
    group = HEADS // KV_HEADS
    scale = HEAD_DIM ** (-0.5)
    local_heads = query_weight.shape[1] // HEAD_DIM
    kv_count = max(1, local_heads // group)
    share = min(local_heads, group)
    first = lax.axis_index("tp") * local_heads // group
    key_cols = lax.dynamic_slice_in_dim(key_weight, first * HEAD_DIM, kv_count * HEAD_DIM, 1)
    value_cols = lax.dynamic_slice_in_dim(value_weight, first * HEAD_DIM, kv_count * HEAD_DIM, 1)
    joined = jnp.concatenate([query_weight, key_cols, value_cols], axis=1)
    wide = hidden.astype(jnp.float32)
    normed = (
        wide * lax.rsqrt(jnp.mean(wide * wide, axis=-1, keepdims=True) + 1e-06) * norm_gain
    ).astype(jnp.bfloat16)
    projected = jnp.dot(normed, joined, preferred_element_type=jnp.float32).astype(jnp.bfloat16)
    query_width = local_heads * HEAD_DIM
    kv_width = kv_count * HEAD_DIM
    queries = projected[:, :query_width]
    key_value = projected[:, query_width:]
    all_pairs = lax.all_gather(key_value, "sp", axis=0, tiled=True)
    rows = queries.shape[0]
    offset = lax.axis_index("sp") * rows
    span = math.gcd(all_pairs.shape[0], 1024)
    turns = (offset + rows + span - 1) // span
    grouped = queries.reshape(rows, kv_count, share, HEAD_DIM)
    bias = head_bias.reshape(kv_count, share)
    query_pos = offset + jnp.arange(rows, dtype=jnp.int32)
    width = 128
    pieces = span // width
    inner = jnp.arange(width, dtype=jnp.int32)
    inner_later = (inner[:, None] > inner[None, :]).astype(jnp.float32)
    outer = jnp.arange(pieces, dtype=jnp.int32)
    outer_later = (outer[:, None] > outer[None, :]).astype(jnp.float32)

    def sweep(turn, carry):
        total, kept = carry
        start = (turns - 1 - turn) * span
        pair_block = lax.dynamic_slice_in_dim(all_pairs, start, span, 0)
        key_block = pair_block[:, :kv_width].reshape(span, kv_count, HEAD_DIM)
        value_block = pair_block[:, kv_width:].reshape(span, kv_count, HEAD_DIM)
        z = (
            jnp.einsum("qgrd,kgd->grqk", grouped, key_block, preferred_element_type=jnp.float32)
            * scale
        )
        z = z + bias[:, :, None, None]
        key_pos = start + jnp.arange(span, dtype=jnp.int32)
        strict = (key_pos[None, :] < query_pos[:, None])[None, None, :, :]
        keep = jnp.where(strict, jax.nn.log_sigmoid(-z), 0.0)
        split_keep = keep.reshape(kv_count, share, rows, pieces, width)
        within = jnp.einsum(
            "grqpj,js->grqps", split_keep, inner_later, precision=lax.Precision.HIGHEST
        )
        piece_sums = jnp.sum(split_keep, axis=4)
        later = jnp.einsum(
            "grqj,jp->grqp", piece_sums, outer_later, precision=lax.Precision.HIGHEST
        )
        between = (within + later[..., None]).reshape(kv_count, share, rows, span) + kept[..., None]
        weight = jnp.where(strict, jnp.exp(jax.nn.log_sigmoid(z) + between), 0.0).astype(
            jnp.bfloat16
        )
        total = total + jnp.einsum(
            "grqk,kgd->grqd", weight, value_block, preferred_element_type=jnp.float32
        )
        kept = kept + jnp.sum(piece_sums, axis=3)
        return (total, kept)

    start_total = jnp.zeros((kv_count, share, rows, HEAD_DIM), jnp.float32)
    start_kept = jnp.zeros((kv_count, share, rows), jnp.float32)
    total, kept = lax.fori_loop(0, turns, sweep, (start_total, start_kept))
    attended = total.transpose(2, 0, 1, 3).reshape(rows, query_width).astype(jnp.bfloat16)
    every_head = lax.all_gather(attended, "tp", axis=1, tiled=True)
    summed = jnp.dot(
        every_head,
        lax.all_gather(output_weight, "tp", axis=0, tiled=True),
        preferred_element_type=jnp.float32,
    )
    return summed.astype(jnp.bfloat16)


def solution(mesh):
    placed = (P("sp", None), P(), P(None, "tp"), P(), P(), P("tp"), P("tp", None))
    return jax.shard_map(
        local, mesh=mesh, in_specs=placed, out_specs=P("sp", None), check_vma=False
    )
```

profile of v0, /device:TPU:31, one launch (start us, length us, event | category | flops | bytes accessed | tf_op | source)
XLA Modules:
  0.0 212.0 jit_solution(2560538919984444730)
XLA Ops:
  6.5 1.4 fusion.35
  7.9 1.6 constant_dynamic-slice_fusion.1
  9.5 2.7 %fusion.38 = bf16[192,768]{1,0:T(8,128)(2,1)S(1)} fusion(bf16[2048,128]{1,0:T(8,128)(2,1)S(1)} %get-tuple-element.204, bf16[2048,128]{1,0:T(8,128)(2,1)S(1)} %get-tuple-element.205, bf16[2048,512]{1,0:T(8,128)(2,1)} %param.11, bf16[192,2048]{1,0:T(8,128)(2,1)} %param.9, f32[2048]{0:T(1024)} %param.10, f32[192]{0:T(256)S(1)} %add_rsqrt_fusion), kind=kOutput, calls=%fused_computation.48 | convolution fusion | flops 615137280 | bytes 4236032 | tf_op jit(solution)/shard_map/dot_general | solution.py:27
  12.2 0.6 slice.20
  12.9 0.0 all-gather.3.cloned.1.call-update
  12.9 0.0 all-gather.5.cloned.1.call-start
  13.0 0.7 all-gather.5.cloned.1.call-update
  13.7 0.1 copy.16
  13.8 54.4 %all-gather.3.cloned.1.call-done = bf16[3072,256]{1,0:T(8,128)(2,1)} async-done(((bf16[192,256]{1,0:T(8,128)(2,1)}), bf16[3072,256]{1,0:T(8,128)(2,1)}) %all-gather.3.cloned.1.call-update) | async-done | bytes 1572880 | tf_op jit(solution)/shard_map/all_gather | solution.py:32
  68.3 128.9 %while.15 = (s32[]{:T(128)}, f32[2,4,192,64]{2,3,1,0:T(8,128)S(1)}, f32[2,4,192]{2,1,0:T(4,128)S(1)}, s32[]{:T(128)}, s32[]{:T(128)}, /*index=5*/bf16[3072,256]{...) while((s32[]{:T(128)}, f32[2,4,192,64]{2,3,1,0:T(8,128)S(1)}, ...), condition=%wide.region_4.5_spmd.clone, body=%wide.region_1.4_spmd.clone.sunk | while | flops 2862535936 | bytes 73637744 | solution.py:81
  68.3 1.1 constant_dynamic-slice_fusion.4
  69.4 0.1 copy.31
  69.5 0.1 add.240
  69.6 0.2 broadcast_compare_fusion.2
  69.8 0.1 copy.32
  70.0 6.7 %fusion.73 = (f32[2,4,192]{2,1,0:T(4,128)S(1)}, f32[2,4,192,1024]{3,2,1,0:T(8,128)S(1)}, f32[2,1024,192,4]{1,2,3,0:T(8,128)}) fusion(f32[2,4]{1,0:T(2,128)S(1)} %add.240, pred[192,1024]{1,0:T(8,128)(4,1)S(1)} %broadcast_compare_fusion.2, bf16[1024,2,64,1]{0,2,3,1:T(8,128)(2,1)S(1)} %bitcast.89, bf16[192,2,4,64]{0,3,2,1:T(8,128)(2,1)S(1)} %get-tuple-element.308), kind=kOutput, calls=%fused_computation.55.clone.1 | convolution fusion | flops 218626560 | bytes 13244448 | tf_op jit(solution)/shard_map/while/body/qgrd,kgd->grqk/dot_general | solution.py:54
  76.7 4.5 %copy.33 = f32[192,8,8,128]{3,2,1,0:T(8,128)} copy(f32[192,8,8,128]{3,1,2,0:T(8,128)S(1)} %bitcast.87) | data formatting | bytes 12582912 | tf_op jit(solution)/shard_map/while
  81.2 5.5 %reduce_sum.39 = f32[2,4,192,8]{3,2,1,0:T(8,128)S(1)} reduce(f32[2,4,192,8,128]{4,3,2,1,0:T(8,128)} %bitcast.85, f32[]{:T(128)} %constant.73.clone.1..sunk), dimensions={4}, to_apply=%region_2.2 | reduce | flops 1560576 | bytes 6340612 | tf_op jit(solution)/shard_map/while/body/reduce_sum | solution.py:65
  86.7 0.8 fusion.74
  87.5 9.0 %broadcast_add_fusion.2 = f32[2,4,192,8,128]{4,3,2,1,0:T(8,128)} fusion(f32[2,4,192,8]{3,2,1,0:T(8,128)S(1)} %fusion.74, f32[2,4,192,8,128]{4,3,2,1,0:T(8,128)} %bitcast.86), kind=kOutput, calls=%fused_computation.20.clone.1 | convolution fusion | flops 2417524736 | bytes 12632064 | tf_op jit(solution)/shard_map/while/body/grqpj,js->grqps/dot_general | solution.py:62
  96.5 7.1 %reshape.78 = f32[2,4,192,1024]{3,2,1,0:T(8,128)} reshape(f32[2,4,192,8,128]{4,3,2,1,0:T(8,128)} %broadcast_add_fusion.2) | data formatting | bytes 12582912 | tf_op jit(solution)/shard_map/while/body/reshape | solution.py:69
  103.6 8.6 %fusion.75 = f32[2,4,192,64]{2,3,1,0:T(8,128)S(1)} fusion(f32[2,4,192,64]{2,3,1,0:T(8,128)S(1)} %get-tuple-element.288, bf16[1024,2,64,1]{0,2,3,1:T(8,128)(2,1)S(1)} %bitcast.88, f32[2,4,192,1024]{3,2,1,0:T(8,128)} %reshape.78, f32[2,1024,192,4]{1,2,3,0:T(8,128)} %get-tuple-element.270, f32[2,4,192]{2,1,0:T(4,128)S(1)} %get-tuple-element.289, ...), kind=kOutput, calls=%fused_computation.22.clone.1 | convolution fusion | flops 223444992 | bytes 13834272 | tf_op jit(solution)/shard_map/while/body/grqk,kgd->grqd/dot_general | solution.py:73
  112.2 1.1 constant_dynamic-slice_fusion.4
  113.3 0.1 copy.31
  113.4 0.1 add.240
  113.5 0.2 broadcast_compare_fusion.2
  113.7 0.1 copy.32
  113.8 6.7 %fusion.73 = (f32[2,4,192]{2,1,0:T(4,128)S(1)}, f32[2,4,192,1024]{3,2,1,0:T(8,128)S(1)}, f32[2,1024,192,4]{1,2,3,0:T(8,128)}) fusion(f32[2,4]{1,0:T(2,128)S(1)} %add.240, pred[192,1024]{1,0:T(8,128)(4,1)S(1)} %broadcast_compare_fusion.2, bf16[1024,2,64,1]{0,2,3,1:T(8,128)(2,1)S(1)} %bitcast.89, bf16[192,2,4,64]{0,3,2,1:T(8,128)(2,1)S(1)} %get-tuple-element.308), kind=kOutput, calls=%fused_computation.55.clone.1 | convolution fusion | flops 218626560 | bytes 13244448 | tf_op jit(solution)/shard_map/while/body/qgrd,kgd->grqk/dot_general | solution.py:54
  120.5 4.1 %copy.33 = f32[192,8,8,128]{3,2,1,0:T(8,128)} copy(f32[192,8,8,128]{3,1,2,0:T(8,128)S(1)} %bitcast.87) | data formatting | bytes 12582912 | tf_op jit(solution)/shard_map/while
  124.7 4.5 %reduce_sum.39 = f32[2,4,192,8]{3,2,1,0:T(8,128)S(1)} reduce(f32[2,4,192,8,128]{4,3,2,1,0:T(8,128)} %bitcast.85, f32[]{:T(128)} %constant.73.clone.1..sunk), dimensions={4}, to_apply=%region_2.2 | reduce | flops 1560576 | bytes 6340612 | tf_op jit(solution)/shard_map/while/body/reduce_sum | solution.py:65
  129.2 0.8 fusion.74
  130.0 9.0 %broadcast_add_fusion.2 = f32[2,4,192,8,128]{4,3,2,1,0:T(8,128)} fusion(f32[2,4,192,8]{3,2,1,0:T(8,128)S(1)} %fusion.74, f32[2,4,192,8,128]{4,3,2,1,0:T(8,128)} %bitcast.86), kind=kOutput, calls=%fused_computation.20.clone.1 | convolution fusion | flops 2417524736 | bytes 12632064 | tf_op jit(solution)/shard_map/while/body/grqpj,js->grqps/dot_general | solution.py:62
  139.0 7.1 %reshape.78 = f32[2,4,192,1024]{3,2,1,0:T(8,128)} reshape(f32[2,4,192,8,128]{4,3,2,1,0:T(8,128)} %broadcast_add_fusion.2) | data formatting | bytes 12582912 | tf_op jit(solution)/shard_map/while/body/reshape | solution.py:69
  146.1 8.6 %fusion.75 = f32[2,4,192,64]{2,3,1,0:T(8,128)S(1)} fusion(f32[2,4,192,64]{2,3,1,0:T(8,128)S(1)} %get-tuple-element.288, bf16[1024,2,64,1]{0,2,3,1:T(8,128)(2,1)S(1)} %bitcast.88, f32[2,4,192,1024]{3,2,1,0:T(8,128)} %reshape.78, f32[2,1024,192,4]{1,2,3,0:T(8,128)} %get-tuple-element.270, f32[2,4,192]{2,1,0:T(4,128)S(1)} %get-tuple-element.289, ...), kind=kOutput, calls=%fused_computation.22.clone.1 | convolution fusion | flops 223444992 | bytes 13834272 | tf_op jit(solution)/shard_map/while/body/grqk,kgd->grqd/dot_general | solution.py:73
  154.7 1.1 constant_dynamic-slice_fusion.4
  155.8 0.1 copy.31
  155.9 0.1 add.240
  156.0 0.2 broadcast_compare_fusion.2
  156.2 0.1 copy.32
  156.3 6.7 %fusion.73 = (f32[2,4,192]{2,1,0:T(4,128)S(1)}, f32[2,4,192,1024]{3,2,1,0:T(8,128)S(1)}, f32[2,1024,192,4]{1,2,3,0:T(8,128)}) fusion(f32[2,4]{1,0:T(2,128)S(1)} %add.240, pred[192,1024]{1,0:T(8,128)(4,1)S(1)} %broadcast_compare_fusion.2, bf16[1024,2,64,1]{0,2,3,1:T(8,128)(2,1)S(1)} %bitcast.89, bf16[192,2,4,64]{0,3,2,1:T(8,128)(2,1)S(1)} %get-tuple-element.308), kind=kOutput, calls=%fused_computation.55.clone.1 | convolution fusion | flops 218626560 | bytes 13244448 | tf_op jit(solution)/shard_map/while/body/qgrd,kgd->grqk/dot_general | solution.py:54
  163.1 4.1 %copy.33 = f32[192,8,8,128]{3,2,1,0:T(8,128)} copy(f32[192,8,8,128]{3,1,2,0:T(8,128)S(1)} %bitcast.87) | data formatting | bytes 12582912 | tf_op jit(solution)/shard_map/while
  167.2 4.5 %reduce_sum.39 = f32[2,4,192,8]{3,2,1,0:T(8,128)S(1)} reduce(f32[2,4,192,8,128]{4,3,2,1,0:T(8,128)} %bitcast.85, f32[]{:T(128)} %constant.73.clone.1..sunk), dimensions={4}, to_apply=%region_2.2 | reduce | flops 1560576 | bytes 6340612 | tf_op jit(solution)/shard_map/while/body/reduce_sum | solution.py:65
  171.7 0.8 fusion.74
  172.5 9.0 %broadcast_add_fusion.2 = f32[2,4,192,8,128]{4,3,2,1,0:T(8,128)} fusion(f32[2,4,192,8]{3,2,1,0:T(8,128)S(1)} %fusion.74, f32[2,4,192,8,128]{4,3,2,1,0:T(8,128)} %bitcast.86), kind=kOutput, calls=%fused_computation.20.clone.1 | convolution fusion | flops 2417524736 | bytes 12632064 | tf_op jit(solution)/shard_map/while/body/grqpj,js->grqps/dot_general | solution.py:62
  181.5 7.1 %reshape.78 = f32[2,4,192,1024]{3,2,1,0:T(8,128)} reshape(f32[2,4,192,8,128]{4,3,2,1,0:T(8,128)} %broadcast_add_fusion.2) | data formatting | bytes 12582912 | tf_op jit(solution)/shard_map/while/body/reshape | solution.py:69
  188.6 8.6 %fusion.75 = f32[2,4,192,64]{2,3,1,0:T(8,128)S(1)} fusion(f32[2,4,192,64]{2,3,1,0:T(8,128)S(1)} %get-tuple-element.288, bf16[1024,2,64,1]{0,2,3,1:T(8,128)(2,1)S(1)} %bitcast.88, f32[2,4,192,1024]{3,2,1,0:T(8,128)} %reshape.78, f32[2,1024,192,4]{1,2,3,0:T(8,128)} %get-tuple-element.270, f32[2,4,192]{2,1,0:T(4,128)S(1)} %get-tuple-element.289, ...), kind=kOutput, calls=%fused_computation.22.clone.1 | convolution fusion | flops 223444992 | bytes 13834272 | tf_op jit(solution)/shard_map/while/body/grqk,kgd->grqd/dot_general | solution.py:73
  197.2 3.9 %all_gather.10 = bf16[192,1024]{0,1:T(8,128)(2,1)S(1)} all-gather(bf16[192,512]{0,1:T(8,128)(2,1)S(1)} %bitcast.90), channel_id=1, replica_groups=mesh['sp'=16,'tp'=2] {'tp'}, dimensions={1}, use_global_device_ids=true | all-gather | bytes 589824 | tf_op jit(solution)/shard_map/all_gather | solution.py:83
  201.1 4.1 %convolution_convert_fusion = bf16[192,2048]{1,0:T(8,128)(2,1)} fusion(bf16[192,1024]{0,1:T(8,128)(2,1)S(1)} %all_gather.10, bf16[1024,2048]{1,0:T(8,128)(2,1)} %all-gather.5.cloned.1.call-done), kind=kOutput, calls=%fused_computation.42 | convolution fusion | flops 805699584 | bytes 5373952 | tf_op jit(solution)/shard_map/dot_general | solution.py:84
  (18 shorter events, 0.2 us)
Async XLA Ops:
  6.5 61.7 %all-gather.3.cloned.1.call-start = ((), (), s32[]{:S(2)}) async-start(), calls=%async_computation | async-start | bytes 1671168 | tf_op jit(solution)/shard_map/all_gather | solution.py:32
  9.5 58.8 %copy-start = (f32[8]{0:T(128)S(1)}, f32[8]{0:T(128)}, u32[]{:S(2)}) copy-start(f32[8]{0:T(128)} %param.14) | copy-start | bytes 100
  12.9 188.2 %all-gather.5.cloned.1.call-start = ((), (), s32[]{:S(2)}) async-start(), calls=%async_computation.1 | async-start | bytes 6291456 | tf_op jit(solution)/shard_map/all_gather | solution.py:86
Sparse Core Ops, SparseCore 0:
  13.0 55.1 all-gather.2
  69.8 17.1 all-gather.4
where the time goes:
time: 214 us; the launch traced here: 212 us
  matrix products  82 us (38%)
  waiting for transfers between devices  55.1 us (26%)
  local copies, waits for them, and re-layouts  40.9 us (19%)
  other arithmetic  16.5 us (8%)
  between operations  13.5 us (6%)
  blocking collectives  3.85 us (2%)
    all_gather x1, waiting for transfers between devices, local(): all_pairs = lax.all_gather(key_value, 'sp', axis=0, tiled=True)  54.4 us
    dot_general x3, matrix products, sweep(): jnp.einsum('grqpj,js->grqps', split_keep, inner_later, precision=lax.Prec...  27 us
    dot_general x3, matrix products, sweep(): jnp.einsum('grqk,kgd->grqd', weight, value_block, preferred_element_type=...  25.7 us
    reshape x3, local copies, waits for them, and re-layouts, sweep(): (within + later[..., None]).reshape(kv_count, share, rows, span)  21.3 us
    dot_general x3, matrix products, sweep(): jnp.einsum('qgrd,kgd->grqk', grouped, key_block, preferred_element_type=j...  20.1 us
    reduce_sum x3, other arithmetic, sweep(): piece_sums = jnp.sum(split_keep, axis=4)  14.5 us
    while x9, local copies, waits for them, and re-layouts  13.7 us
  transfers between devices with their start and end apart: 2, of which 1 were waited for; matrix products, arithmetic and copies ran while one was open for 61% of the time, Pallas kernels for 0%

commit v1 on v0

v1 whole, which is shorter than its diff:
```python
import functools
import math

import jax
import jax.numpy as jnp
from jax import lax
from jax.experimental import pallas as pl
from jax.experimental.pallas import tpu as pltpu
from jax.sharding import PartitionSpec as P

HEADS = 16
KV_HEADS = 4
HEAD_DIM = 64
LOG2E = math.log2(math.e)


def attend_kernel(span, kv_count, share, bias_ref, q_ref, pairs_ref, out_ref, heads_q, total, kept, tri):
    rows = q_ref.shape[0]
    heads = kv_count * share
    kv_width = kv_count * HEAD_DIM
    offset = lax.axis_index("sp") * rows
    for h in range(heads):
        heads_q[h] = q_ref[:, h * HEAD_DIM : (h + 1) * HEAD_DIM]
    total[...] = jnp.zeros_like(total)
    kept[...] = jnp.zeros_like(kept)
    above = lax.broadcasted_iota(jnp.int32, (span, span), 0)
    below = lax.broadcasted_iota(jnp.int32, (span, span), 1)
    tri[...] = (above > below).astype(jnp.float32).astype(jnp.bfloat16)

    def chunk(start, masked):
        start = pl.multiple_of(start, span)
        block = pairs_ref[pl.ds(start, span), :]
        if masked:
            key_pos = start + lax.broadcasted_iota(jnp.int32, (rows, span), 1)
            query_pos = offset + lax.broadcasted_iota(jnp.int32, (rows, span), 0)
            strict = key_pos < query_pos
        later = tri[...]
        for g in range(kv_count):
            key_block = block[:, g * HEAD_DIM : (g + 1) * HEAD_DIM]
            value_block = block[:, kv_width + g * HEAD_DIM : kv_width + (g + 1) * HEAD_DIM]
            for r in range(share):
                h = g * share + r
                dots = lax.dot_general(
                    heads_q[h], key_block, (((1,), (1,)), ((), ())), preferred_element_type=jnp.float32
                )
                u = dots * (HEAD_DIM ** (-0.5) * LOG2E) + bias_ref[h] * LOG2E
                drop = jnp.maximum(u, jnp.log2(1.0 + jnp.exp2(jnp.minimum(u, 126.0))))
                if masked:
                    drop = jnp.where(strict, drop, 0.0)
                after = jnp.dot(drop.astype(jnp.bfloat16), later, preferred_element_type=jnp.float32)
                before = kept[h][:, :1]
                power = (u - drop) - (after + before)
                weight = jnp.exp2(power)
                if masked:
                    weight = jnp.where(strict, weight, 0.0)
                total[h] += jnp.dot(
                    weight.astype(jnp.bfloat16), value_block, preferred_element_type=jnp.float32
                )
                kept[h] = jnp.broadcast_to(before + (after[:, :1] + drop[:, :1]), kept.shape[1:])

    whole = offset // span
    turns = (offset + rows + span - 1) // span

    def edge(turn, _):
        chunk((turns - 1 - turn) * span, True)
        return 0

    def plain(turn, _):
        chunk((whole - 1 - turn) * span, False)
        return 0

    lax.fori_loop(0, turns - whole, edge, 0)
    lax.fori_loop(0, whole, plain, 0)
    for h in range(heads):
        out_ref[:, h * HEAD_DIM : (h + 1) * HEAD_DIM] = total[h].astype(jnp.bfloat16)


def local(hidden, norm_gain, query_weight, key_weight, value_weight, head_bias, output_weight):
    group = HEADS // KV_HEADS
    local_heads = query_weight.shape[1] // HEAD_DIM
    kv_count = max(1, local_heads // group)
    share = min(local_heads, group)
    first = lax.axis_index("tp") * local_heads // group
    key_cols = lax.dynamic_slice_in_dim(key_weight, first * HEAD_DIM, kv_count * HEAD_DIM, 1)
    value_cols = lax.dynamic_slice_in_dim(value_weight, first * HEAD_DIM, kv_count * HEAD_DIM, 1)
    wide = hidden.astype(jnp.float32)
    normed = (
        wide * lax.rsqrt(jnp.mean(wide * wide, axis=-1, keepdims=True) + 1e-06) * norm_gain
    ).astype(jnp.bfloat16)
    joined = jnp.concatenate([key_cols, value_cols], axis=1)
    key_value = jnp.dot(normed, joined, preferred_element_type=jnp.float32).astype(jnp.bfloat16)
    all_pairs = lax.all_gather(key_value, "sp", axis=0, tiled=True)
    queries = jnp.dot(normed, query_weight, preferred_element_type=jnp.float32).astype(jnp.bfloat16)
    rows = queries.shape[0]
    span = math.gcd(all_pairs.shape[0], 256)
    heads = local_heads
    attended = pl.pallas_call(
        functools.partial(attend_kernel, span, kv_count, share),
        out_shape=jax.ShapeDtypeStruct((rows, heads * HEAD_DIM), jnp.bfloat16),
        in_specs=[
            pl.BlockSpec(memory_space=pltpu.SMEM),
            pl.BlockSpec(memory_space=pltpu.VMEM),
            pl.BlockSpec(memory_space=pltpu.VMEM),
        ],
        out_specs=pl.BlockSpec(memory_space=pltpu.VMEM),
        scratch_shapes=[
            pltpu.VMEM((heads, rows, HEAD_DIM), jnp.bfloat16),
            pltpu.VMEM((heads, rows, HEAD_DIM), jnp.float32),
            pltpu.VMEM((heads, rows, 128), jnp.float32),
            pltpu.VMEM((span, span), jnp.bfloat16),
        ],
        cost_estimate=pl.CostEstimate(flops=2000000000, bytes_accessed=4000000, transcendentals=10000000),
    )(head_bias, queries, all_pairs)
    every_head = lax.all_gather(attended, "tp", axis=1, tiled=True)
    summed = jnp.dot(
        every_head,
        lax.all_gather(output_weight, "tp", axis=0, tiled=True),
        preferred_element_type=jnp.float32,
    )
    return summed.astype(jnp.bfloat16)


def solution(mesh):
    placed = (P("sp", None), P(), P(None, "tp"), P(), P(), P("tp"), P("tp", None))
    return jax.shard_map(
        local, mesh=mesh, in_specs=placed, out_specs=P("sp", None), check_vma=False
    )
```

time: 214 us -> 107 us (0.50)
  matrix products: 82 us -> 6.46 us
  local copies, waits for them, and re-layouts: 40.9 us -> 1.6 us
  Pallas kernels: 0 us -> 24.1 us
  other arithmetic: 16.5 us -> 1.53 us
    dot_general x12 -> x1, matrix products: 75.2 us -> 1.31 us  [local(): jnp.dot(normed, query_weight, preferred_element_type=jnp.float32)]
    pallas_call x0 -> x1, Pallas kernels: none -> 24.1 us  [local(): pl.pallas_call(functools.partial(attend_kernel, span, kv_count, share), o...]
    reshape x3 -> x0, local copies, waits for them, and re-layouts: 21.3 us -> none  [sweep(): (within + later[..., None]).reshape(kv_count, share, rows, span)]
    reduce_sum x3 -> x0, other arithmetic: 14.5 us -> none  [sweep(): piece_sums = jnp.sum(split_keep, axis=4)]
    while x9 -> x0, local copies, waits for them, and re-layouts: 13.7 us -> none
    slice x6 -> x0, local copies, waits for them, and re-layouts: 4.01 us -> none  [the longest x3 3.21 us: sweep(): key_block = pair_block[:, :kv_width].reshape(span, kv_count, HEAD_DIM)]
  transfers between devices with their start and end apart: 2 -> 2, of which waited for: 1 -> 1; matrix products, arithmetic and copies ran while one was open for 61% -> 1% of each run, Pallas kernels for 0% -> 23%
where the time goes in v1:
time: 107 us; the launch traced here: 106 us
  waiting for transfers between devices  53.9 us (50%)
  Pallas kernels  24.1 us (23%)
  between operations  13.5 us (13%)
  matrix products  6.46 us (6%)
  blocking collectives  4.46 us (4%)
  local copies, waits for them, and re-layouts  1.6 us (1%)
  other arithmetic  1.53 us (1%)
    all_gather x1, waiting for transfers between devices, local(): all_pairs = lax.all_gather(key_value, 'sp', axis=0, tiled=True)  53.2 us
    pallas_call x1, Pallas kernels, local(): pl.pallas_call(functools.partial(attend_kernel, span, kv_count, share), o...  24.1 us
    all_gather x1, blocking collectives, local(): every_head = lax.all_gather(attended, 'tp', axis=1, tiled=True)  4.46 us
    dot_general x1, matrix products, local(): jnp.dot(every_head, lax.all_gather(output_weight, 'tp', axis=0, tiled=Tru...  4.06 us
  transfers between devices with their start and end apart: 2, of which 1 were waited for; matrix products, arithmetic and copies ran while one was open for 1% of the time, Pallas kernels for 23%

profile of v1, /device:TPU:31, one launch (start us, length us, event | category | flops | bytes accessed | tf_op | source)
XLA Modules:
  0.0 105.6 jit_solution(16866115154932126063)
XLA Ops:
  6.5 0.0 copy-start
  6.5 0.0 copy-start.1
  6.5 0.0 copy-start.2
  6.5 0.0 all-gather.3.cloned.1.call-start
  6.6 1.5 %fusion = f32[192]{0:T(256)S(1)} fusion(bf16[192,2048]{1,0:T(8,128)(2,1)} %param.7), kind=kLoop, calls=%fused_computation.3 | loop fusion | flops 1179456 | bytes 787200 | tf_op jit(solution)/shard_map/reduce_sum | solution.py:88
  8.1 1.6 %constant_dynamic-slice_fusion = (bf16[2048,128]{1,0:T(8,128)(2,1)S(1)}, bf16[2048,128]{1,0:T(8,128)(2,1)S(1)}) fusion(bf16[2048,256]{1,0:T(8,128)(2,1)} %param.11, s32[]{:T(128)S(6)} %select_n.10, bf16[2048,256]{1,0:T(8,128)(2,1)} %param.10), kind=kLoop, calls=%fused_computation.12 | loop fusion | bytes 2097156 | tf_op jit(solution)/shard_map/dynamic_slice | solution.py:85
  9.7 0.0 copy-done.1
  9.7 0.0 copy-done.2
  9.7 1.1 %convolution_convert_fusion.2 = bf16[192,256]{1,0:T(8,128)(2,1)} fusion(bf16[2048,128]{1,0:T(8,128)(2,1)S(1)} %get-tuple-element.5, bf16[2048,128]{1,0:T(8,128)(2,1)S(1)} %get-tuple-element.6, bf16[192,2048]{1,0:T(8,128)(2,1)S(1)} %copy-done.1, f32[2048]{0:T(1024)S(1)} %copy-done.2, f32[192]{0:T(256)S(1)} %add_rsqrt_fusion), kind=kOutput, calls=%fused_computation.7 | convolution fusion | flops 205045760 | bytes 1942272 | tf_op jit(solution)/shard_map/dot_general | solution.py:91
  10.8 0.0 all-gather.3.cloned.1.call-update
  10.8 0.0 all-gather.5.cloned.1.call-start
  10.9 0.7 all-gather.5.cloned.1.call-update
  11.6 0.0 copy-done
  11.6 1.3 %convolution_convert_fusion.1.q_ref = bf16[192,512]{1,0:T(8,128)(2,1)} fusion(bf16[2048,512]{1,0:T(8,128)(2,1)S(1)} %copy-done, bf16[192,2048]{1,0:T(8,128)(2,1)S(1)} %copy-done.1, f32[2048]{0:T(1024)S(1)} %copy-done.2, f32[192]{0:T(256)S(1)} %add_rsqrt_fusion), kind=kOutput, calls=%fused_computation.6 | convolution fusion | flops 404324352 | bytes 3089152 | tf_op jit(solution)/shard_map/dot_general | solution.py:93
  12.9 53.2 %all-gather.3.cloned.1.call-done.pairs_ref = bf16[3072,256]{1,0:T(8,128)(2,1)} async-done(((bf16[192,256]{1,0:T(8,128)(2,1)}), bf16[3072,256]{1,0:T(8,128)(2,1)}) %all-gather.3.cloned.1.call-update) | async-done | bytes 1572880 | tf_op jit(solution)/shard_map/all_gather | solution.py:92
  66.1 24.1 %shard_map.73 = bf16[192,512]{1,0:T(8,128)(2,1)} custom-call(f32[8]{0:T(128)} %bias_ref.1, bf16[192,512]{1,0:T(8,128)(2,1)} %convolution_convert_fusion.1.q_ref, bf16[3072,256]{1,0:T(8,128)(2,1)} %all-gather.3.cloned.1.call-done.pairs_ref), custom_call_target="tpu_custom_call" | custom-call | flops 2000000000 | bytes 4000000 | tf_op jit(solution)/shard_map/pallas_call | solution.py:97
  90.2 4.5 %all_gather.10 = bf16[192,1024]{1,0:T(8,128)(2,1)S(1)} all-gather(bf16[192,512]{1,0:T(8,128)(2,1)} %shard_map.73), channel_id=1, replica_groups=mesh['sp'=16,'tp'=2] {'tp'}, dimensions={1}, use_global_device_ids=true | all-gather | bytes 589824 | tf_op jit(solution)/shard_map/all_gather | solution.py:114
  94.7 0.0 all-gather.5.cloned.1.call-done
  94.7 4.1 %convolution_convert_fusion = bf16[192,2048]{1,0:T(8,128)(2,1)} fusion(bf16[192,1024]{1,0:T(8,128)(2,1)S(1)} %all_gather.10, bf16[1024,2048]{1,0:T(8,128)(2,1)} %all-gather.5.cloned.1.call-done), kind=kOutput, calls=%fused_computation | convolution fusion | flops 805699584 | bytes 5373952 | tf_op jit(solution)/shard_map/dot_general | solution.py:115
  (1 shorter events, 0.0 us)
Async XLA Ops:
  6.5 5.1 %copy-start = (bf16[2048,512]{1,0:T(8,128)(2,1)S(1)}, bf16[2048,512]{1,0:T(8,128)(2,1)}, u32[]{:S(2)}) copy-start(bf16[2048,512]{1,0:T(8,128)(2,1)} %param.9) | copy-start | bytes 6291460
  6.5 3.2 %copy-start.1 = (bf16[192,2048]{1,0:T(8,128)(2,1)S(1)}, bf16[192,2048]{1,0:T(8,128)(2,1)}, u32[]{:S(2)}) copy-start(bf16[192,2048]{1,0:T(8,128)(2,1)} %param.7) | copy-start | bytes 2359300
  6.5 3.2 %copy-start.2 = (f32[2048]{0:T(1024)S(1)}, f32[2048]{0:T(1024)}, u32[]{:S(2)}) copy-start(f32[2048]{0:T(1024)} %param.8) | copy-start | bytes 24580
  6.5 59.6 %all-gather.3.cloned.1.call-start = ((), (), s32[]{:S(2)}) async-start(), calls=%async_computation | async-start | bytes 1671168 | tf_op jit(solution)/shard_map/all_gather | solution.py:92
  10.8 83.9 %all-gather.5.cloned.1.call-start = ((), (), s32[]{:S(2)}) async-start(), calls=%async_computation.1 | async-start | bytes 6291456 | tf_op jit(solution)/shard_map/all_gather | solution.py:117
Sparse Core Ops, SparseCore 0:
  11.0 55.1 all-gather.2
  67.6 17.1 all-gather.4

commit v2 on v1

v2 whole, which is shorter than its diff:
```python
import functools
import math

import jax
import jax.numpy as jnp
from jax import lax
from jax.experimental import pallas as pl
from jax.experimental.pallas import tpu as pltpu
from jax.sharding import PartitionSpec as P

HEADS = 16
KV_HEADS = 4
HEAD_DIM = 64
LOG2E = math.log2(math.e)


PLANE = 4
MESH = pl.DeviceIdType.MESH


def layer_kernel(
    span, kv_count, share, devices, ranks,
    bias_ref, q_ref, kv_ref, mix_ref, out_ref,
    pairs, spare, heads_q, total, kept, tri, gathered, mixers,
    arrive, spare_arrive, up_sem, side_sem, over_sem, own_sem, mix_send, mix_arrive, mix_local, att_send, att_arrive,
):
    rows = q_ref.shape[0]
    heads = kv_count * share
    kv_width = kv_count * HEAD_DIM
    me = lax.axis_index("sp")
    rank = lax.axis_index("tp")
    levels = devices // PLANE
    level = me // PLANE
    place = me % PLANE
    across = PLANE - 1 - place
    side = place + 1 - 2 * (place % 2)
    over = (place + 2) % PLANE
    has_up = level < levels - 1
    offset = me * rows

    def slot(block):
        return pairs.at[pl.ds(pl.multiple_of(block * rows, 16), rows), :]

    def ship(source, block, send, target):
        return pltpu.make_async_remote_copy(
            src_ref=source, dst_ref=slot(block), send_sem=send, recv_sem=arrive.at[block],
            device_id={"sp": target}, device_id_type=MESH,
        )

    def own_to(index, where):
        return ship(kv_ref, me, own_sem.at[index], level * PLANE + where)

    def own_spare():
        return pltpu.make_async_remote_copy(
            src_ref=kv_ref, dst_ref=spare, send_sem=own_sem.at[2], recv_sem=spare_arrive,
            device_id={"sp": level * PLANE + across}, device_id_type=MESH,
        )

    def lift_up():
        return ship(spare, level * PLANE + across, up_sem.at[level * PLANE + across], me + PLANE)

    def own_up():
        return ship(kv_ref, me, up_sem.at[me], me + PLANE)

    def send_up(block):
        return ship(slot(block), block, up_sem.at[block], me + PLANE)

    def send_side(block):
        return ship(slot(block), block, side_sem.at[block], level * PLANE + side)

    def send_over(block):
        return ship(slot(block), block, over_sem.at[block], level * PLANE + over)

    def mixer(step):
        return pltpu.make_async_remote_copy(
            src_ref=mix_ref, dst_ref=mixers.at[rank], send_sem=mix_send.at[step],
            recv_sem=mix_arrive.at[step], device_id={"tp": (rank + step) % ranks}, device_id_type=MESH,
        )

    def attended(step):
        return pltpu.make_async_remote_copy(
            src_ref=gathered.at[rank], dst_ref=gathered.at[rank], send_sem=att_send.at[step],
            recv_sem=att_arrive.at[step], device_id={"tp": (rank + step) % ranks}, device_id_type=MESH,
        )

    pl.when(side > place)(lambda: own_to(0, side).start())
    pl.when(over > place)(lambda: own_to(1, over).start())
    pl.when(has_up)(lambda: own_up().start())
    pl.when(across > place)(lambda: own_to(2, across).start())
    pl.when((across < place) & has_up)(lambda: own_spare().start())
    mine = pltpu.make_async_copy(mix_ref, mixers.at[rank], mix_local)
    mine.start()
    for step in range(1, ranks):
        mixer(step).start()

    pairs[pl.ds(pl.multiple_of(offset, 16), rows), :] = kv_ref[...]
    for h in range(heads):
        heads_q[h] = q_ref[:, h * HEAD_DIM : (h + 1) * HEAD_DIM]
    total[...] = jnp.zeros_like(total)
    kept[...] = jnp.zeros_like(kept)
    first_pos = lax.broadcasted_iota(jnp.int32, (span, span), 0)
    second_pos = lax.broadcasted_iota(jnp.int32, (span, span), 1)
    tri[...] = (first_pos > second_pos).astype(jnp.float32).astype(jnp.bfloat16)

    def take(block):
        ship(slot(block), block, up_sem.at[block], (me + 1) % devices).wait_recv()
        spot = block % PLANE
        lower = block // PLANE < level

        def relay_up():
            send_up(block).start()

        def relay_plane():
            send_side(block).start()
            send_over(block).start()

        pl.when(has_up & ((spot == place) | (spot == across)))(relay_up)
        pl.when(lower & (spot == place))(relay_plane)

    def take_until(front, low):
        low = jnp.maximum(low, 0)
        count = jnp.maximum(front - low, 0)

        def one(index, _):
            take(front - 1 - index)
            return 0

        lax.fori_loop(0, count, one, 0)
        return front - count

    def chunk(start, masked):
        start = pl.multiple_of(start, span)
        block = pairs[pl.ds(start, span), :]
        if masked:
            key_pos = start + lax.broadcasted_iota(jnp.int32, (rows, span), 1)
            query_pos = offset + lax.broadcasted_iota(jnp.int32, (rows, span), 0)
            strict = key_pos < query_pos
            value_pos = start + lax.broadcasted_iota(jnp.int32, (span, block.shape[1]), 0)
            block = jnp.where(value_pos < offset + rows, block.astype(jnp.float32), 0.0)
            block = block.astype(jnp.bfloat16)
        later = tri[...]
        for g in range(kv_count):
            key_block = block[:, g * HEAD_DIM : (g + 1) * HEAD_DIM]
            value_block = block[:, kv_width + g * HEAD_DIM : kv_width + (g + 1) * HEAD_DIM]
            for r in range(share):
                h = g * share + r
                dots = lax.dot_general(
                    heads_q[h], key_block, (((1,), (1,)), ((), ())), preferred_element_type=jnp.float32
                )
                u = dots * (HEAD_DIM ** (-0.5) * LOG2E) + bias_ref[h] * LOG2E
                drop = jnp.maximum(u, jnp.log2(1.0 + jnp.exp2(jnp.minimum(u, 126.0))))
                if masked:
                    drop = jnp.where(strict, drop, 0.0)
                after = jnp.dot(drop.astype(jnp.bfloat16), later, preferred_element_type=jnp.float32)
                before = kept[h][:, :1]
                weight = jnp.exp2((u - drop) - (after + before))
                if masked:
                    weight = jnp.where(strict, weight, 0.0)
                total[h] += jnp.dot(
                    weight.astype(jnp.bfloat16), value_block, preferred_element_type=jnp.float32
                )
                kept[h] = jnp.broadcast_to(before + (after[:, :1] + drop[:, :1]), kept.shape[1:])

    whole = offset // span
    turns = (offset + rows + span - 1) // span

    def edge(turn, front):
        start = (turns - 1 - turn) * span
        front = take_until(front, start // rows)
        chunk(start, True)
        return front

    def plain(turn, front):
        start = (whole - 1 - turn) * span
        front = take_until(front, (start - span) // rows)
        chunk(start, False)
        return front

    front = lax.fori_loop(0, turns - whole, edge, me)

    def lift():
        own_spare().wait_recv()
        lift_up().start()

    pl.when(has_up & (across > place))(lift)
    front = lax.fori_loop(0, whole, plain, front)
    take_until(front, 0)

    for h in range(heads):
        gathered[rank, :, h * HEAD_DIM : (h + 1) * HEAD_DIM] = total[h].astype(jnp.bfloat16)
    for step in range(1, ranks):
        attended(step).start()
    mine.wait()
    for step in range(1, ranks):
        mixer(step).wait_recv()
    for step in range(1, ranks):
        attended(step).wait_recv()
    features = out_ref.shape[1]
    tile = math.gcd(features, 512)
    for column in range(0, features, tile):
        summed = jnp.zeros((rows, tile), jnp.float32)
        for r in range(ranks):
            summed += jnp.dot(
                gathered[r], mixers[r, :, column : column + tile], preferred_element_type=jnp.float32
            )
        out_ref[:, column : column + tile] = summed.astype(jnp.bfloat16)

    pl.when(side > place)(lambda: own_to(0, side).wait_send())
    pl.when(over > place)(lambda: own_to(1, over).wait_send())
    pl.when(across > place)(lambda: own_to(2, across).wait_send())
    pl.when((across < place) & has_up)(lambda: own_spare().wait_send())
    pl.when(has_up)(lambda: own_up().wait_send())
    pl.when(has_up & (across > place))(lambda: lift_up().wait_send())

    def settle(block, _):
        spot = block % PLANE
        lower = block // PLANE < level

        def plane_done():
            send_side(block).wait_send()
            send_over(block).wait_send()

        pl.when(has_up & ((spot == place) | (spot == across)))(lambda: send_up(block).wait_send())
        pl.when(lower & (spot == place))(plane_done)
        return 0

    lax.fori_loop(0, me, settle, 0)
    for step in range(1, ranks):
        mixer(step).wait_send()
        attended(step).wait_send()


def local(hidden, norm_gain, query_weight, key_weight, value_weight, head_bias, output_weight):
    group = HEADS // KV_HEADS
    local_heads = query_weight.shape[1] // HEAD_DIM
    kv_count = max(1, local_heads // group)
    share = min(local_heads, group)
    first = lax.axis_index("tp") * local_heads // group
    key_cols = lax.dynamic_slice_in_dim(key_weight, first * HEAD_DIM, kv_count * HEAD_DIM, 1)
    value_cols = lax.dynamic_slice_in_dim(value_weight, first * HEAD_DIM, kv_count * HEAD_DIM, 1)
    wide = hidden.astype(jnp.float32)
    normed = (
        wide * lax.rsqrt(jnp.mean(wide * wide, axis=-1, keepdims=True) + 1e-06) * norm_gain
    ).astype(jnp.bfloat16)
    joined = jnp.concatenate([key_cols, value_cols], axis=1)
    key_value = jnp.dot(normed, joined, preferred_element_type=jnp.float32).astype(jnp.bfloat16)
    queries = jnp.dot(normed, query_weight, preferred_element_type=jnp.float32).astype(jnp.bfloat16)
    rows = queries.shape[0]
    devices = lax.axis_size("sp")
    ranks = lax.axis_size("tp")
    span = math.gcd(rows * devices, 256)
    width = query_weight.shape[1]
    features = output_weight.shape[1]
    vmem = pl.BlockSpec(memory_space=pltpu.VMEM)
    dma = pltpu.SemaphoreType.DMA
    return pl.pallas_call(
        functools.partial(layer_kernel, span, kv_count, share, devices, ranks),
        out_shape=jax.ShapeDtypeStruct((rows, features), jnp.bfloat16),
        in_specs=[
            pl.BlockSpec(memory_space=pltpu.SMEM),
            vmem,
            vmem,
            pl.BlockSpec(memory_space=pl.ANY),
        ],
        out_specs=vmem,
        scratch_shapes=[
            pltpu.VMEM((rows * devices, key_value.shape[1]), jnp.bfloat16),
            pltpu.VMEM(key_value.shape, jnp.bfloat16),
            pltpu.VMEM((local_heads, rows, HEAD_DIM), jnp.bfloat16),
            pltpu.VMEM((local_heads, rows, HEAD_DIM), jnp.float32),
            pltpu.VMEM((local_heads, rows, 128), jnp.float32),
            pltpu.VMEM((span, span), jnp.bfloat16),
            pltpu.VMEM((ranks, rows, width), jnp.bfloat16),
            pltpu.VMEM((ranks, width, features), jnp.bfloat16),
            dma((devices,)),
            dma,
            dma((devices,)),
            dma((devices,)),
            dma((devices,)),
            dma((3,)),
            dma((ranks,)),
            dma((ranks,)),
            dma,
            dma((ranks,)),
            dma((ranks,)),
        ],
        compiler_params=pltpu.CompilerParams(has_side_effects=True),
    )(head_bias, queries, key_value, output_weight)


def solution(mesh):
    placed = (P("sp", None), P(), P(None, "tp"), P(), P(), P("tp"), P("tp", None))
    return jax.shard_map(
        local, mesh=mesh, in_specs=placed, out_specs=P("sp", None), check_vma=False
    )
```

time: 107 us -> 71.7 us (0.67)
  the two profiles are of different devices: /device:TPU:31 before, /device:TPU:27 now
where the time goes in v2:
time: 71.7 us; the launch traced here: 71.4 us
  Pallas kernels  62.7 us (87%)
  matrix products  3.65 us (5%)
  local copies, waits for them, and re-layouts  3.51 us (5%)
  other arithmetic  1.53 us (2%)
    pallas_call x1, Pallas kernels, local(): pl.pallas_call(functools.partial(layer_kernel, span, kv_count, share, dev...  62.7 us
    unnamed x11, local copies, waits for them, and re-layouts  3.11 us
    dot_general x1, matrix products, local(): jnp.dot(normed, query_weight, preferred_element_type=jnp.float32)  2.59 us
    reduce_sum x1, other arithmetic, local(): jnp.mean(wide * wide, axis=-1, keepdims=True) + 1e-06  1.52 us

profile of v2, /device:TPU:27, one launch (start us, length us, event | category | flops | bytes accessed | tf_op | source)
XLA Modules:
  0.0 71.4 jit_solution(9156576627190932972)
XLA Ops:
  0.0 0.0 copy-start
  0.0 1.5 %fusion = f32[192]{0:T(256)S(1)} fusion(bf16[192,2048]{1,0:T(8,128)(2,1)} %param.7), kind=kLoop, calls=%fused_computation.2 | loop fusion | flops 1179456 | bytes 787200 | tf_op jit(solution)/shard_map/reduce_sum | solution.py:243
  1.5 0.3 copy-done
  1.8 0.0 copy-start.2
  1.8 0.0 copy-start.3
  1.8 2.6 %convolution_convert_fusion.q_ref = bf16[192,512]{1,0:T(8,128)(2,1)} fusion(bf16[2048,512]{1,0:T(8,128)(2,1)S(1)} %copy-done, bf16[192,2048]{1,0:T(8,128)(2,1)} %param.7, f32[2048]{0:T(1024)} %param.8, f32[192]{0:T(256)S(1)} %add_rsqrt_fusion), kind=kOutput, calls=%fused_computation.5 | convolution fusion | flops 404324352 | bytes 3089152 | tf_op jit(solution)/shard_map/dot_general | solution.py:247
  4.4 0.0 copy-done.2
  4.4 0.0 copy-done.3
  4.4 0.0 copy-start.1
  4.4 0.0 copy-start.4
  4.4 0.4 constant_dynamic-slice_fusion
  4.9 0.7 copy-done.1
  5.6 0.0 copy-done.4
  5.6 1.1 %convolution_convert_fusion.1.kv_ref = bf16[192,256]{1,0:T(8,128)(2,1)} fusion(bf16[2048,128]{1,0:T(8,128)(2,1)S(1)} %get-tuple-element.5, bf16[2048,128]{1,0:T(8,128)(2,1)S(1)} %get-tuple-element.6, bf16[192,2048]{1,0:T(8,128)(2,1)S(1)} %copy-done.1, f32[2048]{0:T(1024)S(1)} %copy-done.4, f32[192]{0:T(256)S(1)} %add_rsqrt_fusion), kind=kOutput, calls=%fused_computation.6 | convolution fusion | flops 205045760 | bytes 1942272 | tf_op jit(solution)/shard_map/dot_general | solution.py:246
  6.6 62.7 %shard_map.73 = bf16[192,2048]{1,0:T(8,128)(2,1)} custom-call(f32[8]{0:T(128)} %bias_ref.1, bf16[192,512]{1,0:T(8,128)(2,1)} %convolution_convert_fusion.q_ref, bf16[192,256]{1,0:T(8,128)(2,1)} %convolution_convert_fusion.1.kv_ref, bf16[512,2048]{1,0:T(8,128)(2,1)} %mix_ref.1), custom_call_target="tpu_custom_call" | custom-call | tf_op jit(solution)/shard_map/pallas_call | solution.py:256
  69.4 2.1 %copy.9 = bf16[192,2048]{1,0:T(8,128)(2,1)} copy(bf16[192,2048]{1,0:T(8,128)(2,1)} %shard_map.73) | data formatting | bytes 1572864
  (1 shorter events, 0.0 us)
Async XLA Ops:
  0.0 1.8 %copy-start = (bf16[2048,512]{1,0:T(8,128)(2,1)S(1)}, bf16[2048,512]{1,0:T(8,128)(2,1)}, u32[]{:S(2)}) copy-start(bf16[2048,512]{1,0:T(8,128)(2,1)} %param.9) | copy-start | bytes 6291460
  1.8 2.6 %copy-start.2 = (bf16[2048,256]{1,0:T(8,128)(2,1)S(1)}, bf16[2048,256]{1,0:T(8,128)(2,1)}, u32[]{:S(2)}) copy-start(bf16[2048,256]{1,0:T(8,128)(2,1)} %param.11) | copy-start | bytes 3145732
  1.8 2.6 %copy-start.3 = (bf16[2048,256]{1,0:T(8,128)(2,1)S(1)}, bf16[2048,256]{1,0:T(8,128)(2,1)}, u32[]{:S(2)}) copy-start(bf16[2048,256]{1,0:T(8,128)(2,1)} %param.10) | copy-start | bytes 3145732
  4.4 1.1 %copy-start.1 = (bf16[192,2048]{1,0:T(8,128)(2,1)S(1)}, bf16[192,2048]{1,0:T(8,128)(2,1)}, u32[]{:S(2)}) copy-start(bf16[192,2048]{1,0:T(8,128)(2,1)} %param.7) | copy-start | bytes 2359300
  4.4 1.1 %copy-start.4 = (f32[2048]{0:T(1024)S(1)}, f32[2048]{0:T(1024)}, u32[]{:S(2)}) copy-start(f32[2048]{0:T(1024)} %param.8) | copy-start | bytes 24580

commit v3 on v2

--- a/solution.py
+++ b/solution.py
@@ -15,6 +15,7 @@
 
 
 PLANE = 4
+PACE = 2
 MESH = pl.DeviceIdType.MESH
 
 
@@ -102,31 +103,58 @@
     second_pos = lax.broadcasted_iota(jnp.int32, (span, span), 1)
     tri[...] = (first_pos > second_pos).astype(jnp.float32).astype(jnp.bfloat16)
 
-    def take(block):
+    def arrived(block):
         ship(slot(block), block, up_sem.at[block], (me + 1) % devices).wait_recv()
-        spot = block % PLANE
-        lower = block // PLANE < level
-
-        def relay_up():
-            send_up(block).start()
-
-        def relay_plane():
-            send_side(block).start()
-            send_over(block).start()
-
-        pl.when(has_up & ((spot == place) | (spot == across)))(relay_up)
-        pl.when(lower & (spot == place))(relay_plane)
+
+    def relay_column(block):
+        arrived(block)
+        pl.when(has_up)(lambda: send_up(block).start())
+        send_side(block).start()
+        send_over(block).start()
+
+    def relay_across(block):
+        arrived(block)
+        pl.when(has_up)(lambda: send_up(block).start())
+
+    def lift():
+        own_spare().wait_recv()
+        lift_up().start()
+
+    def relay(group):
+        pl.when((group == 0) & has_up & (across > place))(lift)
+        lower = level - group
+        held = lower * PLANE + across
+        pl.when((group > 0) | (across < place))(lambda: relay_across(held))
+        pl.when(lower >= 1)(lambda: relay_column((lower - 1) * PLANE + place))
+
+    def relay_until(done, count):
+        count = jnp.minimum(count, level + 1)
+        ahead = jnp.maximum(count - done, 0)
+
+        def one(index, _):
+            relay(done + index)
+            return 0
+
+        lax.fori_loop(0, ahead, one, 0)
+        return done + ahead
 
     def take_until(front, low):
-        low = jnp.maximum(low, 0)
         count = jnp.maximum(front - low, 0)
 
         def one(index, _):
-            take(front - 1 - index)
+            block = front - 1 - index
+            spot = block % PLANE
+            pl.when((spot != place) & (spot != across))(lambda: arrived(block))
             return 0
 
         lax.fori_loop(0, count, one, 0)
         return front - count
+
+    def advance(state, start, turn):
+        done, front = state
+        low = start // rows
+        done = relay_until(done, jnp.maximum(turn // PACE + 1, level - low // PLANE + 1))
+        return done, take_until(front, low)
 
     def chunk(start, masked):
         start = pl.multiple_of(start, span)
@@ -164,26 +192,21 @@
     whole = offset // span
     turns = (offset + rows + span - 1) // span
 
-    def edge(turn, front):
+    def edge(turn, state):
         start = (turns - 1 - turn) * span
-        front = take_until(front, start // rows)
+        state = advance(state, start, turn)
         chunk(start, True)
-        return front
-
-    def plain(turn, front):
+        return state
+
+    def plain(turn, state):
         start = (whole - 1 - turn) * span
-        front = take_until(front, (start - span) // rows)
+        state = advance(state, start, turn + turns - whole)
         chunk(start, False)
-        return front
-
-    front = lax.fori_loop(0, turns - whole, edge, me)
-
-    def lift():
-        own_spare().wait_recv()
-        lift_up().start()
-
-    pl.when(has_up & (across > place))(lift)
-    front = lax.fori_loop(0, whole, plain, front)
+        return state
+
+    state = lax.fori_loop(0, turns - whole, edge, (0, me))
+    done, front = lax.fori_loop(0, whole, plain, state)
+    relay_until(done, level + 1)
     take_until(front, 0)
 
     for h in range(heads):

time: 71.7 us -> 50.2 us (0.70)
  the two profiles are of different devices: /device:TPU:27 before, /device:TPU:31 now
where the time goes in v3:
time: 50.2 us; the launch traced here: 50 us
  Pallas kernels  41.3 us (82%)
  matrix products  3.65 us (7%)
  local copies, waits for them, and re-layouts  3.51 us (7%)
  other arithmetic  1.53 us (3%)
    pallas_call x1, Pallas kernels, local(): pl.pallas_call(functools.partial(layer_kernel, span, kv_count, share, dev...  41.3 us
    unnamed x11, local copies, waits for them, and re-layouts  3.11 us
    dot_general x1, matrix products, local(): jnp.dot(normed, query_weight, preferred_element_type=jnp.float32)  2.59 us
    reduce_sum x1, other arithmetic, local(): jnp.mean(wide * wide, axis=-1, keepdims=True) + 1e-06  1.52 us
    dot_general x1, matrix products, local(): jnp.dot(normed, joined, preferred_element_type=jnp.float32)  1.06 us

profile of v3, /device:TPU:31, one launch (start us, length us, event | category | flops | bytes accessed | tf_op | source)
XLA Modules:
  0.0 50.0 jit_solution(11210465568463251759)
XLA Ops:
  0.0 0.0 copy-start
  0.0 1.5 %fusion = f32[192]{0:T(256)S(1)} fusion(bf16[192,2048]{1,0:T(8,128)(2,1)} %param.7), kind=kLoop, calls=%fused_computation.2 | loop fusion | flops 1179456 | bytes 787200 | tf_op jit(solution)/shard_map/reduce_sum | solution.py:266
  1.5 0.3 copy-done
  1.8 0.0 copy-start.2
  1.8 0.0 copy-start.3
  1.8 2.6 %convolution_convert_fusion.q_ref = bf16[192,512]{1,0:T(8,128)(2,1)} fusion(bf16[2048,512]{1,0:T(8,128)(2,1)S(1)} %copy-done, bf16[192,2048]{1,0:T(8,128)(2,1)} %param.7, f32[2048]{0:T(1024)} %param.8, f32[192]{0:T(256)S(1)} %add_rsqrt_fusion), kind=kOutput, calls=%fused_computation.5 | convolution fusion | flops 404324352 | bytes 3089152 | tf_op jit(solution)/shard_map/dot_general | solution.py:270
  4.4 0.0 copy-done.2
  4.4 0.0 copy-done.3
  4.4 0.0 copy-start.1
  4.4 0.0 copy-start.4
  4.4 0.4 constant_dynamic-slice_fusion
  4.8 0.7 %copy-done.1 = bf16[192,2048]{1,0:T(8,128)(2,1)S(1)} copy-done((bf16[192,2048]{1,0:T(8,128)(2,1)S(1)}, bf16[192,2048]{1,0:T(8,128)(2,1)}, u32[]{:S(2)}) %copy-start.1) | copy-done | bytes 786456
  5.6 0.0 copy-done.4
  5.6 1.1 %convolution_convert_fusion.1.kv_ref = bf16[192,256]{1,0:T(8,128)(2,1)} fusion(bf16[2048,128]{1,0:T(8,128)(2,1)S(1)} %get-tuple-element.5, bf16[2048,128]{1,0:T(8,128)(2,1)S(1)} %get-tuple-element.6, bf16[192,2048]{1,0:T(8,128)(2,1)S(1)} %copy-done.1, f32[2048]{0:T(1024)S(1)} %copy-done.4, f32[192]{0:T(256)S(1)} %add_rsqrt_fusion), kind=kOutput, calls=%fused_computation.6 | convolution fusion | flops 205045760 | bytes 1942272 | tf_op jit(solution)/shard_map/dot_general | solution.py:269
  6.6 41.3 %shard_map.73 = bf16[192,2048]{1,0:T(8,128)(2,1)} custom-call(f32[8]{0:T(128)} %bias_ref.1, bf16[192,512]{1,0:T(8,128)(2,1)} %convolution_convert_fusion.q_ref, bf16[192,256]{1,0:T(8,128)(2,1)} %convolution_convert_fusion.1.kv_ref, bf16[512,2048]{1,0:T(8,128)(2,1)} %mix_ref.1), custom_call_target="tpu_custom_call" | custom-call | tf_op jit(solution)/shard_map/pallas_call | solution.py:279
  47.9 2.1 %copy.9 = bf16[192,2048]{1,0:T(8,128)(2,1)} copy(bf16[192,2048]{1,0:T(8,128)(2,1)} %shard_map.73) | data formatting | bytes 1572864
  (1 shorter events, 0.0 us)
Async XLA Ops:
  0.0 1.8 %copy-start = (bf16[2048,512]{1,0:T(8,128)(2,1)S(1)}, bf16[2048,512]{1,0:T(8,128)(2,1)}, u32[]{:S(2)}) copy-start(bf16[2048,512]{1,0:T(8,128)(2,1)} %param.9) | copy-start | bytes 6291460
  1.8 2.6 %copy-start.2 = (bf16[2048,256]{1,0:T(8,128)(2,1)S(1)}, bf16[2048,256]{1,0:T(8,128)(2,1)}, u32[]{:S(2)}) copy-start(bf16[2048,256]{1,0:T(8,128)(2,1)} %param.11) | copy-start | bytes 3145732
  1.8 2.6 %copy-start.3 = (bf16[2048,256]{1,0:T(8,128)(2,1)S(1)}, bf16[2048,256]{1,0:T(8,128)(2,1)}, u32[]{:S(2)}) copy-start(bf16[2048,256]{1,0:T(8,128)(2,1)} %param.10) | copy-start | bytes 3145732
  4.4 1.1 %copy-start.1 = (bf16[192,2048]{1,0:T(8,128)(2,1)S(1)}, bf16[192,2048]{1,0:T(8,128)(2,1)}, u32[]{:S(2)}) copy-start(bf16[192,2048]{1,0:T(8,128)(2,1)} %param.7) | copy-start | bytes 2359300
  4.4 1.1 %copy-start.4 = (f32[2048]{0:T(1024)S(1)}, f32[2048]{0:T(1024)}, u32[]{:S(2)}) copy-start(f32[2048]{0:T(1024)} %param.8) | copy-start | bytes 24580

commit v4 on v3

--- a/solution.py
+++ b/solution.py
@@ -16,13 +16,15 @@
 
 PLANE = 4
 PACE = 2
+ROWS = 192
+LAG = 8
 MESH = pl.DeviceIdType.MESH
 
 
 def layer_kernel(
     span, kv_count, share, devices, ranks,
     bias_ref, q_ref, kv_ref, mix_ref, out_ref,
-    pairs, spare, heads_q, total, kept, tri, gathered, mixers,
+    pairs, spare, heads_q, total, kept, gain, lost, tri, gathered, mixers,
     arrive, spare_arrive, up_sem, side_sem, over_sem, own_sem, mix_send, mix_arrive, mix_local, att_send, att_arrive,
 ):
     rows = q_ref.shape[0]
@@ -167,27 +169,44 @@
             block = jnp.where(value_pos < offset + rows, block.astype(jnp.float32), 0.0)
             block = block.astype(jnp.bfloat16)
         later = tri[...]
-        for g in range(kv_count):
-            key_block = block[:, g * HEAD_DIM : (g + 1) * HEAD_DIM]
-            value_block = block[:, kv_width + g * HEAD_DIM : kv_width + (g + 1) * HEAD_DIM]
-            for r in range(share):
-                h = g * share + r
-                dots = lax.dot_general(
-                    heads_q[h], key_block, (((1,), (1,)), ((), ())), preferred_element_type=jnp.float32
-                )
-                u = dots * (HEAD_DIM ** (-0.5) * LOG2E) + bias_ref[h] * LOG2E
-                drop = jnp.maximum(u, jnp.log2(1.0 + jnp.exp2(jnp.minimum(u, 126.0))))
-                if masked:
-                    drop = jnp.where(strict, drop, 0.0)
-                after = jnp.dot(drop.astype(jnp.bfloat16), later, preferred_element_type=jnp.float32)
-                before = kept[h][:, :1]
-                weight = jnp.exp2((u - drop) - (after + before))
-                if masked:
-                    weight = jnp.where(strict, weight, 0.0)
-                total[h] += jnp.dot(
-                    weight.astype(jnp.bfloat16), value_block, preferred_element_type=jnp.float32
-                )
-                kept[h] = jnp.broadcast_to(before + (after[:, :1] + drop[:, :1]), kept.shape[1:])
+        scale = HEAD_DIM ** (-0.5) * LOG2E
+        tiles = [(h, t) for h in range(heads) for t in range(0, rows, ROWS)]
+
+        def first(h, t):
+            g = h // share
+            dots = lax.dot_general(
+                heads_q[h, t : t + ROWS], block[:, g * HEAD_DIM : (g + 1) * HEAD_DIM],
+                (((1,), (1,)), ((), ())), preferred_element_type=jnp.float32,
+            )
+            u = dots * scale + bias_ref[h] * LOG2E
+            drop = jnp.maximum(u, jnp.log2(1.0 + jnp.exp2(jnp.minimum(u, 126.0))))
+            if masked:
+                drop = jnp.where(strict[t : t + ROWS], drop, 0.0)
+            gain[h, t : t + ROWS] = u - drop
+            lost[h, t : t + ROWS] = drop.astype(jnp.bfloat16)
+            return drop[:, :1]
+
+        def second(h, t, head):
+            g = h // share
+            part = slice(t, t + ROWS)
+            after = jnp.dot(lost[h, part], later, preferred_element_type=jnp.float32)
+            weight = jnp.exp2(gain[h, part] - (after + jnp.tile(kept[h, part], (1, span // 128))))
+            if masked:
+                weight = jnp.where(strict[part], weight, 0.0)
+            kept[h, part] += jnp.broadcast_to(after[:, :1] + head, (ROWS, 128))
+            total[h, part] += jnp.dot(
+                weight.astype(jnp.bfloat16),
+                block[:, kv_width + g * HEAD_DIM : kv_width + (g + 1) * HEAD_DIM],
+                preferred_element_type=jnp.float32,
+            )
+
+        waiting = []
+        for h, t in tiles:
+            waiting.append((h, t, first(h, t)))
+            if len(waiting) > LAG:
+                second(*waiting.pop(0))
+        for item in waiting:
+            second(*item)
 
     whole = offset // span
     turns = (offset + rows + span - 1) // span
@@ -292,6 +311,8 @@
             pltpu.VMEM((local_heads, rows, HEAD_DIM), jnp.bfloat16),
             pltpu.VMEM((local_heads, rows, HEAD_DIM), jnp.float32),
             pltpu.VMEM((local_heads, rows, 128), jnp.float32),
+            pltpu.VMEM((local_heads, rows, span), jnp.float32),
+            pltpu.VMEM((local_heads, rows, span), jnp.bfloat16),
             pltpu.VMEM((span, span), jnp.bfloat16),
             pltpu.VMEM((ranks, rows, width), jnp.bfloat16),
             pltpu.VMEM((ranks, width, features), jnp.bfloat16),

time: 50.2 us -> 46.2 us (0.920)
  Pallas kernels: 41.3 us -> 37.2 us
    pallas_call x1, Pallas kernels: 41.3 us -> 37.2 us  [local(): pl.pallas_call(functools.partial(layer_kernel, span, kv_count, share, dev...]
where the time goes in v4:
time: 46.2 us; the launch traced here: 45.9 us
  Pallas kernels  37.2 us (81%)
  matrix products  3.65 us (8%)
  local copies, waits for them, and re-layouts  3.51 us (8%)
  other arithmetic  1.53 us (3%)
    pallas_call x1, Pallas kernels, local(): pl.pallas_call(functools.partial(layer_kernel, span, kv_count, share, dev...  37.2 us
    unnamed x11, local copies, waits for them, and re-layouts  3.11 us
    dot_general x1, matrix products, local(): jnp.dot(normed, query_weight, preferred_element_type=jnp.float32)  2.59 us
    reduce_sum x1, other arithmetic, local(): jnp.mean(wide * wide, axis=-1, keepdims=True) + 1e-06  1.52 us
    dot_general x1, matrix products, local(): jnp.dot(normed, joined, preferred_element_type=jnp.float32)  1.06 us

profile of v4, /device:TPU:31, one launch (start us, length us, event | category | flops | bytes accessed | tf_op | source)
XLA Modules:
  0.0 45.9 jit_solution(6288345058253429959)
XLA Ops:
  0.0 0.0 copy-start
  0.0 1.5 %fusion = f32[192]{0:T(256)S(1)} fusion(bf16[192,2048]{1,0:T(8,128)(2,1)} %param.7), kind=kLoop, calls=%fused_computation.2 | loop fusion | flops 1179456 | bytes 787200 | tf_op jit(solution)/shard_map/reduce_sum | solution.py:285
  1.5 0.3 copy-done
  1.8 0.0 copy-start.2
  1.8 0.0 copy-start.3
  1.8 2.6 %convolution_convert_fusion.q_ref = bf16[192,512]{1,0:T(8,128)(2,1)} fusion(bf16[2048,512]{1,0:T(8,128)(2,1)S(1)} %copy-done, bf16[192,2048]{1,0:T(8,128)(2,1)} %param.7, f32[2048]{0:T(1024)} %param.8, f32[192]{0:T(256)S(1)} %add_rsqrt_fusion), kind=kOutput, calls=%fused_computation.5 | convolution fusion | flops 404324352 | bytes 3089152 | tf_op jit(solution)/shard_map/dot_general | solution.py:289
  4.4 0.0 copy-done.2
  4.4 0.0 copy-done.3
  4.4 0.0 copy-start.1
  4.4 0.0 copy-start.4
  4.4 0.4 constant_dynamic-slice_fusion
  4.8 0.7 %copy-done.1 = bf16[192,2048]{1,0:T(8,128)(2,1)S(1)} copy-done((bf16[192,2048]{1,0:T(8,128)(2,1)S(1)}, bf16[192,2048]{1,0:T(8,128)(2,1)}, u32[]{:S(2)}) %copy-start.1) | copy-done | bytes 786456
  5.6 0.0 copy-done.4
  5.6 1.1 %convolution_convert_fusion.1.kv_ref = bf16[192,256]{1,0:T(8,128)(2,1)} fusion(bf16[2048,128]{1,0:T(8,128)(2,1)S(1)} %get-tuple-element.5, bf16[2048,128]{1,0:T(8,128)(2,1)S(1)} %get-tuple-element.6, bf16[192,2048]{1,0:T(8,128)(2,1)S(1)} %copy-done.1, f32[2048]{0:T(1024)S(1)} %copy-done.4, f32[192]{0:T(256)S(1)} %add_rsqrt_fusion), kind=kOutput, calls=%fused_computation.6 | convolution fusion | flops 205045760 | bytes 1942272 | tf_op jit(solution)/shard_map/dot_general | solution.py:288
  6.6 37.2 %shard_map.73 = bf16[192,2048]{1,0:T(8,128)(2,1)} custom-call(f32[8]{0:T(128)} %bias_ref.1, bf16[192,512]{1,0:T(8,128)(2,1)} %convolution_convert_fusion.q_ref, bf16[192,256]{1,0:T(8,128)(2,1)} %convolution_convert_fusion.1.kv_ref, bf16[512,2048]{1,0:T(8,128)(2,1)} %mix_ref.1), custom_call_target="tpu_custom_call" | custom-call | tf_op jit(solution)/shard_map/pallas_call | solution.py:298
  43.8 2.1 %copy.9 = bf16[192,2048]{1,0:T(8,128)(2,1)} copy(bf16[192,2048]{1,0:T(8,128)(2,1)} %shard_map.73) | data formatting | bytes 1572864
  (1 shorter events, 0.0 us)
Async XLA Ops:
  0.0 1.8 %copy-start = (bf16[2048,512]{1,0:T(8,128)(2,1)S(1)}, bf16[2048,512]{1,0:T(8,128)(2,1)}, u32[]{:S(2)}) copy-start(bf16[2048,512]{1,0:T(8,128)(2,1)} %param.9) | copy-start | bytes 6291460
  1.8 2.6 %copy-start.2 = (bf16[2048,256]{1,0:T(8,128)(2,1)S(1)}, bf16[2048,256]{1,0:T(8,128)(2,1)}, u32[]{:S(2)}) copy-start(bf16[2048,256]{1,0:T(8,128)(2,1)} %param.11) | copy-start | bytes 3145732
  1.8 2.6 %copy-start.3 = (bf16[2048,256]{1,0:T(8,128)(2,1)S(1)}, bf16[2048,256]{1,0:T(8,128)(2,1)}, u32[]{:S(2)}) copy-start(bf16[2048,256]{1,0:T(8,128)(2,1)} %param.10) | copy-start | bytes 3145732
  4.4 1.1 %copy-start.1 = (bf16[192,2048]{1,0:T(8,128)(2,1)S(1)}, bf16[192,2048]{1,0:T(8,128)(2,1)}, u32[]{:S(2)}) copy-start(bf16[192,2048]{1,0:T(8,128)(2,1)} %param.7) | copy-start | bytes 2359300
  4.4 1.1 %copy-start.4 = (f32[2048]{0:T(1024)S(1)}, f32[2048]{0:T(1024)}, u32[]{:S(2)}) copy-start(f32[2048]{0:T(1024)} %param.8) | copy-start | bytes 24580

commit v5 on v4

--- a/solution.py
+++ b/solution.py
@@ -23,11 +23,11 @@
 
 def layer_kernel(
     span, kv_count, share, devices, ranks,
-    bias_ref, q_ref, kv_ref, mix_ref, out_ref,
+    bias_ref, normed_ref, qw_ref, kv_ref, mix_ref, out_ref,
     pairs, spare, heads_q, total, kept, gain, lost, tri, gathered, mixers,
     arrive, spare_arrive, up_sem, side_sem, over_sem, own_sem, mix_send, mix_arrive, mix_local, att_send, att_arrive,
 ):
-    rows = q_ref.shape[0]
+    rows = normed_ref.shape[0]
     heads = kv_count * share
     kv_width = kv_count * HEAD_DIM
     me = lax.axis_index("sp")
@@ -86,19 +86,37 @@
             recv_sem=att_arrive.at[step], device_id={"tp": (rank + step) % ranks}, device_id_type=MESH,
         )
 
+    barrier = pltpu.get_barrier_semaphore()
+
+    def greet(**where):
+        pl.semaphore_signal(barrier, inc=1, device_id=where, device_id_type=MESH)
+
+    for where in (side, over, across):
+        greet(sp=level * PLANE + where)
+    for step in range(1, ranks):
+        greet(tp=(rank + step) % ranks)
+    pl.when(has_up)(lambda: greet(sp=me + PLANE))
+    pl.when(level > 0)(lambda: greet(sp=me - PLANE))
+    pl.semaphore_wait(
+        barrier, 2 + ranks + jnp.minimum(level, 1) + jnp.minimum(levels - 1 - level, 1)
+    )
+
+    pl.when(has_up)(lambda: own_up().start())
+    pl.when((across > place) & has_up)(lambda: own_to(2, across).start())
+    pl.when((across < place) & has_up)(lambda: own_spare().start())
     pl.when(side > place)(lambda: own_to(0, side).start())
     pl.when(over > place)(lambda: own_to(1, over).start())
-    pl.when(has_up)(lambda: own_up().start())
-    pl.when(across > place)(lambda: own_to(2, across).start())
-    pl.when((across < place) & has_up)(lambda: own_spare().start())
+    pl.when((across > place) & (level == levels - 1))(lambda: own_to(2, across).start())
     mine = pltpu.make_async_copy(mix_ref, mixers.at[rank], mix_local)
     mine.start()
     for step in range(1, ranks):
         mixer(step).start()
 
     pairs[pl.ds(pl.multiple_of(offset, 16), rows), :] = kv_ref[...]
+    queries = jnp.dot(normed_ref[...], qw_ref[...], preferred_element_type=jnp.float32)
+    queries = queries.astype(jnp.bfloat16)
     for h in range(heads):
-        heads_q[h] = q_ref[:, h * HEAD_DIM : (h + 1) * HEAD_DIM]
+        heads_q[h] = queries[:, h * HEAD_DIM : (h + 1) * HEAD_DIM]
     total[...] = jnp.zeros_like(total)
     kept[...] = jnp.zeros_like(kept)
     first_pos = lax.broadcasted_iota(jnp.int32, (span, span), 0)
@@ -123,11 +141,11 @@
         lift_up().start()
 
     def relay(group):
-        pl.when((group == 0) & has_up & (across > place))(lift)
         lower = level - group
         held = lower * PLANE + across
+        pl.when(lower >= 1)(lambda: relay_column((lower - 1) * PLANE + place))
+        pl.when((group == 0) & has_up & (across > place))(lift)
         pl.when((group > 0) | (across < place))(lambda: relay_across(held))
-        pl.when(lower >= 1)(lambda: relay_column((lower - 1) * PLANE + place))
 
     def relay_until(done, count):
         count = jnp.minimum(count, level + 1)
@@ -286,8 +304,7 @@
     ).astype(jnp.bfloat16)
     joined = jnp.concatenate([key_cols, value_cols], axis=1)
     key_value = jnp.dot(normed, joined, preferred_element_type=jnp.float32).astype(jnp.bfloat16)
-    queries = jnp.dot(normed, query_weight, preferred_element_type=jnp.float32).astype(jnp.bfloat16)
-    rows = queries.shape[0]
+    rows = normed.shape[0]
     devices = lax.axis_size("sp")
     ranks = lax.axis_size("tp")
     span = math.gcd(rows * devices, 256)
@@ -300,6 +317,7 @@
         out_shape=jax.ShapeDtypeStruct((rows, features), jnp.bfloat16),
         in_specs=[
             pl.BlockSpec(memory_space=pltpu.SMEM),
+            vmem,
             vmem,
             vmem,
             pl.BlockSpec(memory_space=pl.ANY),
@@ -328,8 +346,8 @@
             dma((ranks,)),
             dma((ranks,)),
         ],
-        compiler_params=pltpu.CompilerParams(has_side_effects=True),
-    )(head_bias, queries, key_value, output_weight)
+        compiler_params=pltpu.CompilerParams(has_side_effects=True, collective_id=0),
+    )(head_bias, normed, query_weight, key_value, output_weight)
 
 
 def solution(mesh):

time: 46.2 us -> 38.1 us (0.82)
  Pallas kernels: 37.2 us -> 31.3 us
  matrix products: 3.65 us -> 1.04 us
  other arithmetic: 1.53 us -> 2.91 us
  local copies, waits for them, and re-layouts: 3.51 us -> 2.5 us
    pallas_call x1, Pallas kernels: 37.2 us -> 31.3 us  [local(): pl.pallas_call(functools.partial(layer_kernel, span, kv_count, share, dev...]
    dot_general x1 -> x0, matrix products: 2.59 us -> none  [local(): jnp.dot(normed, query_weight, preferred_element_type=jnp.float32)]
    convert_element_type x0 -> x1, other arithmetic: none -> 1.39 us  [local(): normed = (wide * lax.rsqrt(jnp.mean(wide * wide, axis=-1, keepdims=True)...]
    unnamed x11 -> x7, local copies, waits for them, and re-layouts: 3.11 us -> 2.1 us
where the time goes in v5:
time: 38.1 us; the launch traced here: 37.8 us
  Pallas kernels  31.3 us (82%)
  other arithmetic  2.91 us (8%)
  local copies, waits for them, and re-layouts  2.5 us (7%)
  matrix products  1.04 us (3%)
    pallas_call x1, Pallas kernels, local(): pl.pallas_call(functools.partial(layer_kernel, span, kv_count, share, dev...  31.3 us
    unnamed x7, local copies, waits for them, and re-layouts  2.1 us
    reduce_sum x1, other arithmetic, local(): jnp.mean(wide * wide, axis=-1, keepdims=True) + 1e-06  1.52 us
    convert_element_type x1, other arithmetic, local(): normed = (wide * lax.rsqrt(jnp.mean(wide * wide, axis=-1, keepdims=True)...  1.39 us
    dot_general x1, matrix products, local(): jnp.dot(normed, joined, preferred_element_type=jnp.float32)  1.04 us

profile of v5, /device:TPU:31, one launch (start us, length us, event | category | flops | bytes accessed | tf_op | source)
XLA Modules:
  0.0 37.8 jit_solution(3501579052426225808)
XLA Ops:
  0.0 0.0 copy-start.1
  0.0 0.0 copy-start.2
  0.0 1.5 %fusion = f32[192]{0:T(256)S(1)} fusion(bf16[192,2048]{1,0:T(8,128)(2,1)} %param.7), kind=kLoop, calls=%fused_computation.2 | loop fusion | flops 1179456 | bytes 787200 | tf_op jit(solution)/shard_map/reduce_sum | solution.py:303
  1.5 1.4 %fusion.2.normed_ref = bf16[192,2048]{1,0:T(8,128)(2,1)S(1)} fusion(bf16[192,2048]{1,0:T(8,128)(2,1)} %param.7, f32[2048]{0:T(1024)} %param.8, f32[192]{0:T(256)S(1)} %add_rsqrt_fusion), kind=kLoop, calls=%fused_computation.4 | loop fusion | flops 1572864 | bytes 1581824 | tf_op jit(solution)/shard_map/convert_element_type | solution.py:304
  2.9 0.0 copy-done.1
  2.9 0.0 copy-done.2
  2.9 0.0 copy-start
  3.0 0.4 %constant_dynamic-slice_fusion = (bf16[2048,128]{1,0:T(8,128)(2,1)S(1)}, bf16[2048,128]{1,0:T(8,128)(2,1)S(1)}) fusion(bf16[2048,256]{1,0:T(8,128)(2,1)S(1)} %copy-done.1, s32[]{:T(128)S(6)} %select_n.10, bf16[2048,256]{1,0:T(8,128)(2,1)S(1)} %copy-done.2), kind=kLoop, calls=%fused_computation.10 | loop fusion | bytes 2097156 | tf_op jit(solution)/shard_map/dynamic_slice | solution.py:300
  3.4 1.0 %convolution_convert_fusion.kv_ref = bf16[192,256]{1,0:T(8,128)(2,1)} fusion(bf16[192,2048]{1,0:T(8,128)(2,1)S(1)} %fusion.2.normed_ref, bf16[2048,128]{1,0:T(8,128)(2,1)S(1)} %get-tuple-element.5, bf16[2048,128]{1,0:T(8,128)(2,1)S(1)} %get-tuple-element.6), kind=kOutput, calls=%fused_computation.5 | convolution fusion | flops 203472896 | bytes 1933312 | tf_op jit(solution)/shard_map/dot_general | solution.py:306
  4.4 0.0 copy-done
  4.4 31.3 %shard_map.73 = bf16[192,2048]{1,0:T(8,128)(2,1)} custom-call(f32[8]{0:T(128)} %bias_ref.1, bf16[192,2048]{1,0:T(8,128)(2,1)} %copy-done, bf16[2048,512]{1,0:T(8,128)(2,1)} %qw_ref.1, bf16[192,256]{1,0:T(8,128)(2,1)} %convolution_convert_fusion.kv_ref, bf16[512,2048]{1,0:T(8,128)(2,1)} %mix_ref.1), custom_call_target="tpu_custom_call" | custom-call | tf_op jit(solution)/shard_map/pallas_call | solution.py:315
  35.8 2.1 %copy.9 = bf16[192,2048]{1,0:T(8,128)(2,1)} copy(bf16[192,2048]{1,0:T(8,128)(2,1)} %shard_map.73) | data formatting | bytes 1572864
  (1 shorter events, 0.0 us)
Async XLA Ops:
  0.0 2.9 %copy-start.1 = (bf16[2048,256]{1,0:T(8,128)(2,1)S(1)}, bf16[2048,256]{1,0:T(8,128)(2,1)}, u32[]{:S(2)}) copy-start(bf16[2048,256]{1,0:T(8,128)(2,1)} %param.11) | copy-start | bytes 3145732
  0.0 2.9 %copy-start.2 = (bf16[2048,256]{1,0:T(8,128)(2,1)S(1)}, bf16[2048,256]{1,0:T(8,128)(2,1)}, u32[]{:S(2)}) copy-start(bf16[2048,256]{1,0:T(8,128)(2,1)} %param.10) | copy-start | bytes 3145732
  2.9 1.5 %copy-start = (bf16[192,2048]{1,0:T(8,128)(2,1)}, bf16[192,2048]{1,0:T(8,128)(2,1)S(1)}, u32[]{:S(2)}) copy-start(bf16[192,2048]{1,0:T(8,128)(2,1)S(1)} %fusion.2.normed_ref) | copy-start | bytes 2359300

commit v6 on v5

--- a/solution.py
+++ b/solution.py
@@ -23,11 +23,11 @@
 
 def layer_kernel(
     span, kv_count, share, devices, ranks,
-    bias_ref, normed_ref, qw_ref, kv_ref, mix_ref, out_ref,
-    pairs, spare, heads_q, total, kept, gain, lost, tri, gathered, mixers,
+    bias_ref, hidden_ref, gain_ref, qw_ref, kvw_ref, mix_ref, out_ref,
+    pairs, spare, normed_ref, kv_ref, heads_q, total, kept, gain, lost, tri, gathered, mixers,
     arrive, spare_arrive, up_sem, side_sem, over_sem, own_sem, mix_send, mix_arrive, mix_local, att_send, att_arrive,
 ):
-    rows = normed_ref.shape[0]
+    rows = hidden_ref.shape[0]
     heads = kv_count * share
     kv_width = kv_count * HEAD_DIM
     me = lax.axis_index("sp")
@@ -97,6 +97,13 @@
         greet(tp=(rank + step) % ranks)
     pl.when(has_up)(lambda: greet(sp=me + PLANE))
     pl.when(level > 0)(lambda: greet(sp=me - PLANE))
+    wide = hidden_ref[...].astype(jnp.float32)
+    normed = wide * lax.rsqrt(jnp.mean(wide * wide, axis=-1, keepdims=True) + 1e-06) * gain_ref[...]
+    normed_ref[...] = normed.astype(jnp.bfloat16)
+    key_value = jnp.dot(normed_ref[...], kvw_ref[...], preferred_element_type=jnp.float32)
+    key_value = key_value.astype(jnp.bfloat16)
+    kv_ref[...] = key_value
+    pairs[pl.ds(pl.multiple_of(offset, 16), rows), :] = key_value
     pl.semaphore_wait(
         barrier, 2 + ranks + jnp.minimum(level, 1) + jnp.minimum(levels - 1 - level, 1)
     )
@@ -112,7 +119,6 @@
     for step in range(1, ranks):
         mixer(step).start()
 
-    pairs[pl.ds(pl.multiple_of(offset, 16), rows), :] = kv_ref[...]
     queries = jnp.dot(normed_ref[...], qw_ref[...], preferred_element_type=jnp.float32)
     queries = queries.astype(jnp.bfloat16)
     for h in range(heads):
@@ -298,13 +304,8 @@
     first = lax.axis_index("tp") * local_heads // group
     key_cols = lax.dynamic_slice_in_dim(key_weight, first * HEAD_DIM, kv_count * HEAD_DIM, 1)
     value_cols = lax.dynamic_slice_in_dim(value_weight, first * HEAD_DIM, kv_count * HEAD_DIM, 1)
-    wide = hidden.astype(jnp.float32)
-    normed = (
-        wide * lax.rsqrt(jnp.mean(wide * wide, axis=-1, keepdims=True) + 1e-06) * norm_gain
-    ).astype(jnp.bfloat16)
     joined = jnp.concatenate([key_cols, value_cols], axis=1)
-    key_value = jnp.dot(normed, joined, preferred_element_type=jnp.float32).astype(jnp.bfloat16)
-    rows = normed.shape[0]
+    rows = hidden.shape[0]
     devices = lax.axis_size("sp")
     ranks = lax.axis_size("tp")
     span = math.gcd(rows * devices, 256)
@@ -320,12 +321,15 @@
             vmem,
             vmem,
             vmem,
+            vmem,
             pl.BlockSpec(memory_space=pl.ANY),
         ],
         out_specs=vmem,
         scratch_shapes=[
-            pltpu.VMEM((rows * devices, key_value.shape[1]), jnp.bfloat16),
-            pltpu.VMEM(key_value.shape, jnp.bfloat16),
+            pltpu.VMEM((rows * devices, joined.shape[1]), jnp.bfloat16),
+            pltpu.VMEM((rows, joined.shape[1]), jnp.bfloat16),
+            pltpu.VMEM(hidden.shape, jnp.bfloat16),
+            pltpu.VMEM((rows, joined.shape[1]), jnp.bfloat16),
             pltpu.VMEM((local_heads, rows, HEAD_DIM), jnp.bfloat16),
             pltpu.VMEM((local_heads, rows, HEAD_DIM), jnp.float32),
             pltpu.VMEM((local_heads, rows, 128), jnp.float32),
@@ -347,7 +351,7 @@
             dma((ranks,)),
         ],
         compiler_params=pltpu.CompilerParams(has_side_effects=True, collective_id=0),
-    )(head_bias, normed, query_weight, key_value, output_weight)
+    )(head_bias, hidden, norm_gain[None, :], query_weight, joined, output_weight)
 
 
 def solution(mesh):

time: 38.1 us -> 36.8 us (0.966)
  other arithmetic: 2.91 us -> 1.1 us
  local copies, waits for them, and re-layouts: 2.5 us -> 3.67 us
  matrix products: 1.04 us -> 0 us
  Pallas kernels: 31.3 us -> 31.8 us
    reduce_sum x1 -> x0, other arithmetic: 1.52 us -> none  [local(): jnp.mean(wide * wide, axis=-1, keepdims=True) + 1e-06]
    convert_element_type x1 -> x0, other arithmetic: 1.39 us -> none  [local(): normed = (wide * lax.rsqrt(jnp.mean(wide * wide, axis=-1, keepdims=True)...]
    dynamic_slice x1, local copies, waits for them, and re-layouts: 0.4 us -> 1.58 us  [local(): lax.dynamic_slice_in_dim(value_weight, first * HEAD_DIM, kv_count * HEAD_...]
    concatenate x0 -> x1, other arithmetic: none -> 1.1 us  [local(): joined = jnp.concatenate([key_cols, value_cols], axis=1)]
    dot_general x1 -> x0, matrix products: 1.04 us -> none  [local(): jnp.dot(normed, joined, preferred_element_type=jnp.float32)]
    pallas_call x1, Pallas kernels: 31.3 us -> 31.8 us  [local(): pl.pallas_call(functools.partial(layer_kernel, span, kv_count, share, dev...]
    unnamed x7 -> x1, local copies, waits for them, and re-layouts: 2.1 us -> 2.09 us
where the time goes in v6:
time: 36.8 us; the launch traced here: 36.6 us
  Pallas kernels  31.8 us (86%)
  local copies, waits for them, and re-layouts  3.67 us (10%)
  other arithmetic  1.1 us (3%)
    pallas_call x1, Pallas kernels, local(): pl.pallas_call(functools.partial(layer_kernel, span, kv_count, share, dev...  31.8 us
    unnamed x1, local copies, waits for them, and re-layouts  2.09 us
    dynamic_slice x1, local copies, waits for them, and re-layouts, local(): lax.dynamic_slice_in_dim(value_weight, first * HEAD_DIM, kv_count * HEAD_...  1.58 us
    concatenate x1, other arithmetic, local(): joined = jnp.concatenate([key_cols, value_cols], axis=1)  1.1 us

profile of v6, /device:TPU:31, one launch (start us, length us, event | category | flops | bytes accessed | tf_op | source)
XLA Modules:
  0.0 36.6 jit_solution(11057748531624752290)
XLA Ops:
  0.0 1.6 %constant_dynamic-slice_fusion = (bf16[2048,128]{1,0:T(8,128)(2,1)S(1)}, bf16[2048,128]{1,0:T(8,128)(2,1)S(1)}) fusion(bf16[2048,256]{1,0:T(8,128)(2,1)} %param.11, s32[]{:T(128)S(6)} %select_n.10, bf16[2048,256]{1,0:T(8,128)(2,1)} %param.10), kind=kLoop, calls=%fused_computation.1 | loop fusion | bytes 2097156 | tf_op jit(solution)/shard_map/dynamic_slice | solution.py:306
  1.6 1.1 %pad_maximum_fusion.kvw_ref = bf16[2048,256]{1,0:T(8,128)(2,1)} fusion(bf16[2048,128]{1,0:T(8,128)(2,1)S(1)} %get-tuple-element.5, bf16[2048,128]{1,0:T(8,128)(2,1)S(1)} %get-tuple-element.6), kind=kLoop, calls=%fused_computation | loop fusion | flops 2097152 | bytes 2097152 | tf_op jit(solution)/shard_map/concatenate | solution.py:307
  2.7 31.8 %shard_map.73 = bf16[192,2048]{1,0:T(8,128)(2,1)} custom-call(f32[8]{0:T(128)} %bias_ref.1, bf16[192,2048]{1,0:T(8,128)(2,1)} %hidden_ref.1, f32[1,2048]{1,0:T(1,128)} %bitcast.1, bf16[2048,512]{1,0:T(8,128)(2,1)} %qw_ref.1, bf16[2048,256]{1,0:T(8,128)(2,1)} %pad_maximum_fusion.kvw_ref, bf16[512,2048]{1,0:T(8,128)(2,1)} %mix_ref.1), custom_call_target="tpu_custom_call" | custom-call | tf_op jit(solution)/shard_map/pallas_call | solution.py:316
  34.5 2.1 %copy.9 = bf16[192,2048]{1,0:T(8,128)(2,1)} copy(bf16[192,2048]{1,0:T(8,128)(2,1)} %shard_map.73) | data formatting | bytes 1572864

commit v7 on v6

--- a/solution.py
+++ b/solution.py
@@ -22,10 +22,10 @@
 
 
 def layer_kernel(
-    span, kv_count, share, devices, ranks,
-    bias_ref, hidden_ref, gain_ref, qw_ref, kvw_ref, mix_ref, out_ref,
-    pairs, spare, normed_ref, kv_ref, heads_q, total, kept, gain, lost, tri, gathered, mixers,
-    arrive, spare_arrive, up_sem, side_sem, over_sem, own_sem, mix_send, mix_arrive, mix_local, att_send, att_arrive,
+    span, kv_count, share, devices, ranks, sliced,
+    bias_ref, hidden_ref, gain_ref, qw_hbm, kw_hbm, vw_hbm, mix_ref, out_ref,
+    pairs, spare, normed_ref, kv_ref, qw_ref, kvw_ref, heads_q, total, kept, gain, lost, tri, gathered, mixers,
+    arrive, spare_arrive, up_sem, side_sem, over_sem, own_sem, mix_send, mix_arrive, mix_local, att_send, att_arrive, load_sem,
 ):
     rows = hidden_ref.shape[0]
     heads = kv_count * share
@@ -86,6 +86,23 @@
             recv_sem=att_arrive.at[step], device_id={"tp": (rank + step) % ranks}, device_id_type=MESH,
         )
 
+    if sliced:
+        column = pl.multiple_of(rank * kv_width, kv_width)
+        loads = [
+            pltpu.make_async_copy(
+                source.at[:, pl.ds(column, kv_width)],
+                kvw_ref.at[:, pl.ds(index * kv_width, kv_width)],
+                load_sem.at[index],
+            )
+            for index, source in enumerate((kw_hbm, vw_hbm))
+        ]
+    else:
+        loads = [pltpu.make_async_copy(kw_hbm, kvw_ref, load_sem.at[0])]
+    query_load = pltpu.make_async_copy(qw_hbm, qw_ref, load_sem.at[2])
+    for load in loads:
+        load.start()
+    query_load.start()
+
     barrier = pltpu.get_barrier_semaphore()
 
     def greet(**where):
@@ -100,6 +117,8 @@
     wide = hidden_ref[...].astype(jnp.float32)
     normed = wide * lax.rsqrt(jnp.mean(wide * wide, axis=-1, keepdims=True) + 1e-06) * gain_ref[...]
     normed_ref[...] = normed.astype(jnp.bfloat16)
+    for load in loads:
+        load.wait()
     key_value = jnp.dot(normed_ref[...], kvw_ref[...], preferred_element_type=jnp.float32)
     key_value = key_value.astype(jnp.bfloat16)
     kv_ref[...] = key_value
@@ -119,6 +138,7 @@
     for step in range(1, ranks):
         mixer(step).start()
 
+    query_load.wait()
     queries = jnp.dot(normed_ref[...], qw_ref[...], preferred_element_type=jnp.float32)
     queries = queries.astype(jnp.bfloat16)
     for h in range(heads):
@@ -301,10 +321,15 @@
     local_heads = query_weight.shape[1] // HEAD_DIM
     kv_count = max(1, local_heads // group)
     share = min(local_heads, group)
-    first = lax.axis_index("tp") * local_heads // group
-    key_cols = lax.dynamic_slice_in_dim(key_weight, first * HEAD_DIM, kv_count * HEAD_DIM, 1)
-    value_cols = lax.dynamic_slice_in_dim(value_weight, first * HEAD_DIM, kv_count * HEAD_DIM, 1)
-    joined = jnp.concatenate([key_cols, value_cols], axis=1)
+    kv_width = kv_count * HEAD_DIM
+    sliced = kv_width % 128 == 0 and local_heads % group == 0
+    if sliced:
+        key_side, value_side = key_weight, value_weight
+    else:
+        first = lax.axis_index("tp") * local_heads // group
+        key_cols = lax.dynamic_slice_in_dim(key_weight, first * HEAD_DIM, kv_width, 1)
+        value_cols = lax.dynamic_slice_in_dim(value_weight, first * HEAD_DIM, kv_width, 1)
+        key_side = value_side = jnp.concatenate([key_cols, value_cols], axis=1)
     rows = hidden.shape[0]
     devices = lax.axis_size("sp")
     ranks = lax.axis_size("tp")
@@ -312,24 +337,28 @@
     width = query_weight.shape[1]
     features = output_weight.shape[1]
     vmem = pl.BlockSpec(memory_space=pltpu.VMEM)
+    hbm = pl.BlockSpec(memory_space=pl.ANY)
     dma = pltpu.SemaphoreType.DMA
     return pl.pallas_call(
-        functools.partial(layer_kernel, span, kv_count, share, devices, ranks),
+        functools.partial(layer_kernel, span, kv_count, share, devices, ranks, sliced),
         out_shape=jax.ShapeDtypeStruct((rows, features), jnp.bfloat16),
         in_specs=[
             pl.BlockSpec(memory_space=pltpu.SMEM),
             vmem,
             vmem,
-            vmem,
-            vmem,
-            pl.BlockSpec(memory_space=pl.ANY),
+            hbm,
+            hbm,
+            hbm,
+            hbm,
         ],
         out_specs=vmem,
         scratch_shapes=[
-            pltpu.VMEM((rows * devices, joined.shape[1]), jnp.bfloat16),
-            pltpu.VMEM((rows, joined.shape[1]), jnp.bfloat16),
+            pltpu.VMEM((rows * devices, 2 * kv_width), jnp.bfloat16),
+            pltpu.VMEM((rows, 2 * kv_width), jnp.bfloat16),
             pltpu.VMEM(hidden.shape, jnp.bfloat16),
-            pltpu.VMEM((rows, joined.shape[1]), jnp.bfloat16),
+            pltpu.VMEM((rows, 2 * kv_width), jnp.bfloat16),
+            pltpu.VMEM(query_weight.shape, jnp.bfloat16),
+            pltpu.VMEM((query_weight.shape[0], 2 * kv_width), jnp.bfloat16),
             pltpu.VMEM((local_heads, rows, HEAD_DIM), jnp.bfloat16),
             pltpu.VMEM((local_heads, rows, HEAD_DIM), jnp.float32),
             pltpu.VMEM((local_heads, rows, 128), jnp.float32),
@@ -349,9 +378,10 @@
             dma,
             dma((ranks,)),
             dma((ranks,)),
+            dma((3,)),
         ],
         compiler_params=pltpu.CompilerParams(has_side_effects=True, collective_id=0),
-    )(head_bias, hidden, norm_gain[None, :], query_weight, joined, output_weight)
+    )(head_bias, hidden, norm_gain[None, :], query_weight, key_side, value_side, output_weight)
 
 
 def solution(mesh):

time: 36.8 us -> 33.3 us (0.905)
  local copies, waits for them, and re-layouts: 3.67 us -> 2.09 us
  other arithmetic: 1.1 us -> 0 us
  Pallas kernels: 31.8 us -> 31 us
    dynamic_slice x1 -> x0, local copies, waits for them, and re-layouts: 1.58 us -> none  [local(): lax.dynamic_slice_in_dim(value_weight, first * HEAD_DIM, kv_count * HEAD_...]
    concatenate x1 -> x0, other arithmetic: 1.1 us -> none  [local(): joined = jnp.concatenate([key_cols, value_cols], axis=1)]
    pallas_call x1, Pallas kernels: 31.8 us -> 31 us  [local(): pl.pallas_call(functools.partial(layer_kernel, span, kv_count, share, dev...]
where the time goes in v7:
time: 33.3 us; the launch traced here: 33.1 us
  Pallas kernels  31 us (93%)
  local copies, waits for them, and re-layouts  2.09 us (6%)
    pallas_call x1, Pallas kernels, local(): pl.pallas_call(functools.partial(layer_kernel, span, kv_count, share, dev...  31 us
    unnamed x1, local copies, waits for them, and re-layouts  2.09 us

profile of v7, /device:TPU:31, one launch (start us, length us, event | category | flops | bytes accessed | tf_op | source)
XLA Modules:
  0.0 33.1 jit_solution(8988054081727018493)
XLA Ops:
  0.0 31.0 %shard_map.73 = bf16[192,2048]{1,0:T(8,128)(2,1)} custom-call(f32[8]{0:T(128)} %bias_ref.1, bf16[192,2048]{1,0:T(8,128)(2,1)} %hidden_ref.1, f32[1,2048]{1,0:T(1,128)} %bitcast.1, bf16[2048,512]{1,0:T(8,128)(2,1)} %qw_hbm.1, bf16[2048,256]{1,0:T(8,128)(2,1)} %kw_hbm.1, bf16[2048,256]{1,0:T(8,128)(2,1)} %vw_hbm.1, bf16[512,2048]{1,0:T(8,128)(2,1)} %mix_ref.1), custom_call_target="tpu_custom_call" | custom-call | tf_op jit(solution)/shard_map/pallas_call | solution.py:342
  31.0 2.1 %copy.9 = bf16[192,2048]{1,0:T(8,128)(2,1)} copy(bf16[192,2048]{1,0:T(8,128)(2,1)} %shard_map.73) | data formatting | bytes 1572864

commit v8 on v7

--- a/solution.py
+++ b/solution.py
@@ -15,7 +15,7 @@
 
 
 PLANE = 4
-PACE = 2
+PACE = 3
 ROWS = 192
 LAG = 8
 MESH = pl.DeviceIdType.MESH
@@ -171,7 +171,7 @@
         held = lower * PLANE + across
         pl.when(lower >= 1)(lambda: relay_column((lower - 1) * PLANE + place))
         pl.when((group == 0) & has_up & (across > place))(lift)
-        pl.when((group > 0) | (across < place))(lambda: relay_across(held))
+        pl.when((group > 0) | ((across < place) & has_up))(lambda: relay_across(held))
 
     def relay_until(done, count):
         count = jnp.minimum(count, level + 1)
@@ -190,7 +190,8 @@
         def one(index, _):
             block = front - 1 - index
             spot = block % PLANE
-            pl.when((spot != place) & (spot != across))(lambda: arrived(block))
+            near = (block // PLANE == level) & (level == levels - 1)
+            pl.when((spot != place) & ((spot != across) | near))(lambda: arrived(block))
             return 0
 
         lax.fori_loop(0, count, one, 0)

time: 33.3 us -> 31.8 us (0.955)
  Pallas kernels: 31 us -> 29.6 us
    pallas_call x1, Pallas kernels: 31 us -> 29.6 us  [local(): pl.pallas_call(functools.partial(layer_kernel, span, kv_count, share, dev...]
where the time goes in v8:
time: 31.8 us; the launch traced here: 31.7 us
  Pallas kernels  29.6 us (93%)
  local copies, waits for them, and re-layouts  2.09 us (7%)
    pallas_call x1, Pallas kernels, local(): pl.pallas_call(functools.partial(layer_kernel, span, kv_count, share, dev...  29.6 us
    unnamed x1, local copies, waits for them, and re-layouts  2.09 us

profile of v8, /device:TPU:31, one launch (start us, length us, event | category | flops | bytes accessed | tf_op | source)
XLA Modules:
  0.0 31.7 jit_solution(10049881148302032077)
XLA Ops:
  0.0 29.6 %shard_map.73 = bf16[192,2048]{1,0:T(8,128)(2,1)} custom-call(f32[8]{0:T(128)} %bias_ref.1, bf16[192,2048]{1,0:T(8,128)(2,1)} %hidden_ref.1, f32[1,2048]{1,0:T(1,128)} %bitcast.1, bf16[2048,512]{1,0:T(8,128)(2,1)} %qw_hbm.1, bf16[2048,256]{1,0:T(8,128)(2,1)} %kw_hbm.1, bf16[2048,256]{1,0:T(8,128)(2,1)} %vw_hbm.1, bf16[512,2048]{1,0:T(8,128)(2,1)} %mix_ref.1), custom_call_target="tpu_custom_call" | custom-call | tf_op jit(solution)/shard_map/pallas_call | solution.py:343
  29.6 2.1 %copy.9 = bf16[192,2048]{1,0:T(8,128)(2,1)} copy(bf16[192,2048]{1,0:T(8,128)(2,1)} %shard_map.73) | data formatting | bytes 1572864

commit v9 on v8

--- a/solution.py
+++ b/solution.py
@@ -232,15 +232,19 @@
             return drop[:, :1]
 
         def second(h, t, head):
-            g = h // share
             part = slice(t, t + ROWS)
             after = jnp.dot(lost[h, part], later, preferred_element_type=jnp.float32)
             weight = jnp.exp2(gain[h, part] - (after + jnp.tile(kept[h, part], (1, span // 128))))
             if masked:
                 weight = jnp.where(strict[part], weight, 0.0)
             kept[h, part] += jnp.broadcast_to(after[:, :1] + head, (ROWS, 128))
+            lost[h, part] = weight.astype(jnp.bfloat16)
+
+        def third(h, t):
+            g = h // share
+            part = slice(t, t + ROWS)
             total[h, part] += jnp.dot(
-                weight.astype(jnp.bfloat16),
+                lost[h, part],
                 block[:, kv_width + g * HEAD_DIM : kv_width + (g + 1) * HEAD_DIM],
                 preferred_element_type=jnp.float32,
             )
@@ -252,6 +256,8 @@
                 second(*waiting.pop(0))
         for item in waiting:
             second(*item)
+        for h, t in tiles:
+            third(h, t)
 
     whole = offset // span
     turns = (offset + rows + span - 1) // span

time: 31.8 us -> 31.7 us (level)
  no operation moved by 1% of the time
where the time goes in v9:
time: 31.7 us; the launch traced here: 31.5 us
  Pallas kernels  29.4 us (93%)
  local copies, waits for them, and re-layouts  2.09 us (7%)
    pallas_call x1, Pallas kernels, local(): pl.pallas_call(functools.partial(layer_kernel, span, kv_count, share, dev...  29.4 us
    unnamed x1, local copies, waits for them, and re-layouts  2.09 us

profile of v9, /device:TPU:31, one launch (start us, length us, event | category | flops | bytes accessed | tf_op | source)
XLA Modules:
  0.0 31.5 jit_solution(11196193310775057430)
XLA Ops:
  0.0 29.4 %shard_map.73 = bf16[192,2048]{1,0:T(8,128)(2,1)} custom-call(f32[8]{0:T(128)} %bias_ref.1, bf16[192,2048]{1,0:T(8,128)(2,1)} %hidden_ref.1, f32[1,2048]{1,0:T(1,128)} %bitcast.1, bf16[2048,512]{1,0:T(8,128)(2,1)} %qw_hbm.1, bf16[2048,256]{1,0:T(8,128)(2,1)} %kw_hbm.1, bf16[2048,256]{1,0:T(8,128)(2,1)} %vw_hbm.1, bf16[512,2048]{1,0:T(8,128)(2,1)} %mix_ref.1), custom_call_target="tpu_custom_call" | custom-call | tf_op jit(solution)/shard_map/pallas_call | solution.py:349
  29.4 2.1 %copy.9 = bf16[192,2048]{1,0:T(8,128)(2,1)} copy(bf16[192,2048]{1,0:T(8,128)(2,1)} %shard_map.73) | data formatting | bytes 1572864

commit v10 on v8

--- a/solution.py
+++ b/solution.py
@@ -15,7 +15,7 @@
 
 
 PLANE = 4
-PACE = 3
+PACE = 4
 ROWS = 192
 LAG = 8
 MESH = pl.DeviceIdType.MESH

time: 31.8 us -> 31.9 us (level)
  no operation moved by 1% of the time
where the time goes in v10:
time: 31.9 us; the launch traced here: 31.7 us
  Pallas kernels  29.6 us (93%)
  local copies, waits for them, and re-layouts  2.09 us (7%)
    pallas_call x1, Pallas kernels, local(): pl.pallas_call(functools.partial(layer_kernel, span, kv_count, share, dev...  29.6 us
    unnamed x1, local copies, waits for them, and re-layouts  2.09 us

profile of v10, /device:TPU:31, one launch (start us, length us, event | category | flops | bytes accessed | tf_op | source)
XLA Modules:
  0.0 31.7 jit_solution(13889759268249505484)
XLA Ops:
  0.0 29.6 %shard_map.73 = bf16[192,2048]{1,0:T(8,128)(2,1)} custom-call(f32[8]{0:T(128)} %bias_ref.1, bf16[192,2048]{1,0:T(8,128)(2,1)} %hidden_ref.1, f32[1,2048]{1,0:T(1,128)} %bitcast.1, bf16[2048,512]{1,0:T(8,128)(2,1)} %qw_hbm.1, bf16[2048,256]{1,0:T(8,128)(2,1)} %kw_hbm.1, bf16[2048,256]{1,0:T(8,128)(2,1)} %vw_hbm.1, bf16[512,2048]{1,0:T(8,128)(2,1)} %mix_ref.1), custom_call_target="tpu_custom_call" | custom-call | tf_op jit(solution)/shard_map/pallas_call | solution.py:343
  29.6 2.1 %copy.9 = bf16[192,2048]{1,0:T(8,128)(2,1)} copy(bf16[192,2048]{1,0:T(8,128)(2,1)} %shard_map.73) | data formatting | bytes 1572864
